TPU v7x, 512 devices: a whole 4x4x16 slice. The times are simulated.
512 devices in a mesh: ep: 32 (over z, core), tp: 16 (over y, x).
Axes of the slice: x: 4, y: 4, z: 16, core: 2. Of those that a mesh axis runs over, the one named last changes fastest.
Arguments:
- tokens: bfloat16 [4096, 1024], P('ep', 'tp'), may hold values from -6 to 6
- norm_gain: float32 [1024], replicated, may hold values from 0.1 to 1.9
- gate_weight: bfloat16 [32, 1024, 1024], P('ep', None, 'tp'), may hold values from -0.1875 to 0.1875
- up_weight: bfloat16 [32, 1024, 1024], P('ep', None, 'tp'), may hold values from -0.1875 to 0.1875
- down_weight: bfloat16 [32, 1024, 1024], P('ep', None, 'tp'), may hold values from -0.1875 to 0.1875
- expert_ids: int32 [4096, 4], P('ep'), may hold values from 0 to 31, all different within a row; in each aligned block of 128 rows (0 to 127, 128 to 255, ...) at most 32 rows name the same one
- route_weight: float32 [4096, 4], P('ep'), may hold values from 0.2 to 1
Outputs:
- combined: bfloat16 [4096, 1024], P('ep', 'tp')
Inputs may be any that keep to these rules, and one draw needn't show every extreme that they name: `expert_ids`: each token names 4 different experts; in each aligned block of 128 tokens no expert is named by more than 32 of them, and in some block one expert is named by exactly 32; every expert is named by some token.
All inputs are finite; a program needn't handle non-finite values.
Results may differ from a plain program's by a relative error of at most 0.0035.
Values may be sent and summed in bfloat16 or wider, within the bound.
A program may use at most 64 MiB of HBM per device.

v0:
```python
import jax
import jax.numpy as jnp
from jax import lax
from jax.sharding import Mesh
from jax.sharding import PartitionSpec as P

TP = ("tp_0", "tp_1")


epsilon = 1e-06
swish_alpha = 1.702
clamp_limit = 7.0


def by_axis(shard, axes):
    for axis in axes:
        shard = lax.psum(shard, axis)
    return shard


def whole_of(shard, axes, dim):
    if not axes:
        return shard
    nearer = lax.all_gather(shard, axes[-1], axis=dim, tiled=True)
    return whole_of(nearer, axes[:-1], dim)


def taken_in(shard, axes, dim, take_in, carry):
    everything = jax.tree.map(lambda part: whole_of(part, axes, dim), shard)
    return take_in(carry, everything, jnp.int32(0))


def slot_numbers(flat_ids, expert_count):
    selector = (flat_ids[..., None] == jnp.arange(expert_count, dtype=jnp.int32)).astype(jnp.int32)
    before = jnp.cumsum(selector, axis=-2) - selector
    return jnp.sum(before * selector, axis=-1).astype(jnp.int32)


def by_expert(incoming, ep_count, local_experts):
    capacity = incoming.shape[1]
    width = incoming.shape[2]
    grouped = incoming.reshape(ep_count, local_experts, capacity, width)
    return jnp.transpose(grouped, (1, 0, 2, 3)).reshape(local_experts, ep_count * capacity, width)


def body(tokens, norm_gain, gate_weight, up_weight, down_weight, expert_ids, route_weight):
    tok_rows = expert_ids.shape[0]
    top_count = expert_ids.shape[1]
    local_experts = gate_weight.shape[0]
    ep_count = lax.axis_size("ep")
    expert_total = local_experts * ep_count
    capacity = 2 * tok_rows * top_count // expert_total
    column_width = tokens.shape[1]
    hidden_width = gate_weight.shape[2]
    out_width = down_weight.shape[2]
    flat_ids = expert_ids.reshape(-1).astype(jnp.int32)
    slot_index = slot_numbers(flat_ids, expert_total)
    owner_token = jnp.arange(tok_rows * top_count, dtype=jnp.int32) // top_count
    slot_table = (
        jnp.full((expert_total, capacity), tok_rows, jnp.int32)
        .at[flat_ids, slot_index]
        .set(owner_token)
    )
    full_width = norm_gain.shape[0]
    widened = tokens.astype(jnp.float32)
    square_sum = by_axis(jnp.sum(widened * widened, axis=1), TP)
    inverse = lax.rsqrt(square_sum / full_width + epsilon)
    gain_part = lax.dynamic_slice_in_dim(
        norm_gain, lax.axis_index(TP) * column_width, column_width, 0
    )
    normed = (widened * inverse[:, None] * gain_part.astype(jnp.float32)).astype(jnp.bfloat16)
    padded = jnp.concatenate([normed, jnp.zeros((1, column_width), jnp.bfloat16)], axis=0)
    outgoing = padded[slot_table.reshape(-1)].reshape(expert_total, capacity, column_width)
    incoming = lax.all_to_all(outgoing, "ep", split_axis=0, concat_axis=0, tiled=True)
    row_block = by_expert(incoming, ep_count, local_experts)
    empty = jnp.zeros((local_experts, ep_count * capacity, hidden_width), jnp.float32)

    def add_columns(totals, piece, start):
        gate_rows = lax.dynamic_slice_in_dim(gate_weight, start, piece.shape[2], 1)
        up_rows = lax.dynamic_slice_in_dim(up_weight, start, piece.shape[2], 1)
        gate_part = jnp.einsum("esd,edf->esf", piece, gate_rows, preferred_element_type=jnp.float32)
        up_part = jnp.einsum("esd,edf->esf", piece, up_rows, preferred_element_type=jnp.float32)
        return (totals[0] + gate_part, totals[1] + up_part)

    gate_pre, up_pre = taken_in(row_block, TP, 2, add_columns, (empty, empty))
    gate_pre = jnp.minimum(gate_pre, clamp_limit)
    up_pre = jnp.clip(up_pre, -clamp_limit, clamp_limit)
    hidden = ((up_pre + 1.0) * gate_pre * jax.nn.sigmoid(swish_alpha * gate_pre)).astype(
        jnp.bfloat16
    )
    empty_out = jnp.zeros((local_experts, ep_count * capacity, out_width), jnp.float32)

    def add_hidden(total, piece, start):
        down_rows = lax.dynamic_slice_in_dim(down_weight, start, piece.shape[2], 1)
        return total + jnp.einsum(
            "esf,efd->esd", piece, down_rows, preferred_element_type=jnp.float32
        )

    down_sum = taken_in(hidden, TP, 2, add_hidden, empty_out)
    expert_out = down_sum.astype(jnp.bfloat16).reshape(local_experts, ep_count, capacity, out_width)
    sendback = jnp.transpose(expert_out, (1, 0, 2, 3)).reshape(
        ep_count * local_experts, capacity, out_width
    )
    returned = lax.all_to_all(sendback, "ep", split_axis=0, concat_axis=0, tiled=True)
    flat_back = returned.reshape(expert_total * capacity, out_width)
    picked = (
        flat_back[flat_ids * capacity + slot_index]
        .reshape(tok_rows, top_count, out_width)
        .astype(jnp.float32)
    )
    combined = jnp.sum(picked * route_weight.astype(jnp.float32)[:, :, None], axis=1)
    return combined.astype(jnp.bfloat16)


def solution(mesh):
    split = Mesh(mesh.devices.reshape(mesh.shape["ep"], 4, 4), ("ep", "tp_0", "tp_1"))
    in_specs = (
        P("ep", TP),
        P(),
        P("ep", None, TP),
        P("ep", None, TP),
        P("ep", None, TP),
        P("ep", None),
        P("ep", None),
    )
    out_specs = P("ep", TP)
    return jax.shard_map(body, mesh=split, in_specs=in_specs, out_specs=out_specs, check_vma=False)
```

profile of v0, /device:TPU:1, one launch (start us, length us, event | category | flops | bytes accessed | tf_op | source)
XLA Modules:
  0.0 231.8 jit_solution(11236081657783373569)
XLA Ops:
  6.5 0.8 copy.36
  7.7 0.7 fusion.30
  8.4 9.5 %psum.14 = f32[128]{0:T(128)S(1)} all-reduce(f32[128]{0:T(128)S(1)} %fusion.30), channel_id=1, replica_groups=mesh['ep'=32,'tp_0'=4,'tp_1'=4] {'tp_0'}, use_global_device_ids=true, to_apply=%region_1.2 | all-reduce | flops 128 | bytes 1024 | tf_op jit(solution)/shard_map/psum | solution.py:17
  18.0 8.5 %psum.15 = f32[128]{0:T(128)S(1)} all-reduce(f32[128]{0:T(128)S(1)} %psum.14), channel_id=1, replica_groups=mesh['ep'=32,'tp_0'=4,'tp_1'=4] {'tp_1'}, use_global_device_ids=true, to_apply=%region_2.3 | all-reduce | flops 128 | bytes 1024 | tf_op jit(solution)/shard_map/psum | solution.py:17
  26.5 0.8 dynamic_slice.3
  27.2 0.8 fusion.32
  28.2 1.2 reduce-window.6
  29.7 25.1 %scatter_fusion = s32[32,32]{1,0:T(8,128)S(1)} fusion(s32[32,32]{1,0:T(8,128)S(1)} %broadcast_in_dim.2, s32[512]{0:T(512)S(1)} %bitcast.56, s32[512]{0:T(512)S(1)} %add_select_fusion), kind=kCustom, calls=%fused_computation.2 | custom fusion | bytes 10240 | tf_op jit(solution)/shard_map/scatter | solution.py:62
  55.0 3.2 %gather_fusion = bf16[1024,64]{1,0:T(8,128)(2,1)S(1)} fusion(bf16[129,64]{1,0:T(8,128)(2,1)S(1)} %concatenate.6.clone, s32[1024]{0:T(1024)S(1)} %broadcast_clamp_fusion), kind=kCustom, calls=%fused_computation | custom fusion | bytes 266240 | tf_op jit(solution)/shard_map/gather | solution.py:73
  58.4 35.8 %all_to_all.10 = bf16[32,2,1024]{2,1,0:T(2,128)(2,1)S(1)} all-to-all(bf16[32,2,1024]{2,1,0:T(2,128)(2,1)S(1)} %reshape.199), channel_id=1, replica_groups=mesh['ep'=32,'tp_0'=4,'tp_1'=4] {'ep'}, dimensions={0} | all-to-all | bytes 262144 | tf_op jit(solution)/shard_map/all_to_all | solution.py:74
  94.3 0.2 reshape.200
  94.6 10.6 %all_gather.12 = bf16[1,1024,256]{1,2,0:T(8,128)(2,1)} all-gather(bf16[1,1024,64]{1,2,0:T(8,128)(2,1)S(1)} %copy.41), channel_id=1, replica_groups=mesh['ep'=32,'tp_0'=4,'tp_1'=4] {'tp_1'}, dimensions={2}, use_global_device_ids=true | all-gather | bytes 655360 | tf_op jit(solution)/shard_map/all_gather | solution.py:24
  105.3 29.3 %all-gather.5.cloned.1.call-done = bf16[1,1024,1024]{1,2,0:T(8,128)(2,1)} async-done(((bf16[1,1024,256]{1,2,0:T(8,128)(2,1)}), bf16[1,1024,1024]{1,2,0:T(8,128)(2,1)}) %all-gather.5.cloned.1.call-update) | async-done | bytes 2097168 | tf_op jit(solution)/shard_map/all_gather | solution.py:24
  134.7 2.2 fusion.4
  136.9 0.5 fusion.19
  137.5 12.2 %all-gather = bf16[1024,256]{0,1:T(8,128)(2,1)} all-gather(bf16[1024,64]{0,1:T(8,128)(2,1)S(1)} %fusion.19), channel_id=2, replica_groups=mesh['ep'=32,'tp_0'=4,'tp_1'=4] {'tp_1'}, dimensions={1}, use_global_device_ids=true | all-gather | bytes 655360 | tf_op jit(solution)/shard_map/all_gather | solution.py:24
  149.6 40.4 %all-gather.7.cloned.1.call-done = bf16[1024,1024]{0,1:T(8,128)(2,1)} async-done(((bf16[1024,256]{0,1:T(8,128)(2,1)}), bf16[1024,1024]{0,1:T(8,128)(2,1)}) %all-gather.7.cloned.1.call-update) | async-done | bytes 2097168 | tf_op jit(solution)/shard_map/all_gather | solution.py:24
  190.0 2.1 convolution_convert_fusion
  192.2 0.8 reshape.201
  193.1 13.3 %all-to-all-start.1 = ((bf16[32,2,1024]{2,1,0:T(2,128)(2,1)}), bf16[32,2,1024]{2,1,0:T(2,128)(2,1)S(1)}, u32[]{:S(2)}, u32[]{:S(2)}) async-start(bf16[32,2,1024]{2,1,0:T(2,128)(2,1)} %reshape.201), calls=%async_computation.1 | async-start | bytes 262144 | tf_op jit(solution)/shard_map/all_to_all | solution.py:104
  206.5 15.9 %all-to-all-done.1 = bf16[32,2,1024]{2,1,0:T(2,128)(2,1)S(1)} async-done(((bf16[32,2,1024]{2,1,0:T(2,128)(2,1)}), bf16[32,2,1024]{2,1,0:T(2,128)(2,1)S(1)}, u32[]{:S(2)}, u32[]{:S(2)}) %all-to-all-start.1) | async-done | bytes 131104 | tf_op jit(solution)/shard_map/all_to_all | solution.py:104
  222.6 1.3 gather_fusion.1
  223.9 0.3 fusion.22
  224.2 0.7 copy.44
  (37 shorter events, 1.9 us)
Async XLA Ops:
  6.5 128.1 %copy-start = (bf16[1,1024,64]{1,2,0:T(8,128)(2,1)S(1)}, bf16[1,1024,64]{1,2,0:T(8,128)(2,1)}, u32[]{:S(2)}) copy-start(bf16[1,1024,64]{1,2,0:T(8,128)(2,1)} %param.9) | copy-start | bytes 393220
  6.5 128.1 %all-gather.5.cloned.1.call-start = ((), (), s32[]{:S(2)}) async-start(), calls=%async_computation.2 | async-start | bytes 2621440 | tf_op jit(solution)/shard_map/all_gather | solution.py:24
  94.5 42.4 %copy-start.4 = (bf16[1,1024,64]{1,2,0:T(8,128)(2,1)S(1)}, bf16[1,1024,64]{1,2,0:T(8,128)(2,1)}, u32[]{:S(2)}) copy-start(bf16[1,1024,64]{1,2,0:T(8,128)(2,1)} %param.10) | copy-start | bytes 393220
  105.3 84.7 %all-gather.7.cloned.1.call-start = ((), (), s32[]{:S(2)}) async-start(), calls=%async_computation.3 | async-start | bytes 2621440 | tf_op jit(solution)/shard_map/all_gather | solution.py:24
  134.7 2.2 copy-start.1
  136.9 53.1 %copy-start.2 = (bf16[1,1024,64]{1,2,0:T(8,128)(2,1)S(1)}, bf16[1,1024,64]{1,2,0:T(8,128)(2,1)}, u32[]{:S(2)}) copy-start(bf16[1,1024,64]{1,2,0:T(8,128)(2,1)} %param.11) | copy-start | bytes 393220
  149.6 56.7 %copy-start.3 = (f32[128,4]{0,1:T(4,128)S(1)}, f32[128,4]{0,1:T(4,128)}, u32[]{:S(2)}) copy-start(f32[128,4]{0,1:T(4,128)} %param.13) | copy-start | bytes 6148
  193.1 29.3 %all-to-all-start.1 = ((bf16[32,2,1024]{2,1,0:T(2,128)(2,1)}), bf16[32,2,1024]{2,1,0:T(2,128)(2,1)S(1)}, u32[]{:S(2)}, u32[]{:S(2)}) async-start(bf16[32,2,1024]{2,1,0:T(2,128)(2,1)} %reshape.201), calls=%async_computation.1 | async-start | bytes 262144 | tf_op jit(solution)/shard_map/all_to_all | solution.py:104
Sparse Core Ops, SparseCore 0:
  105.4 29.1 all-gather.4
  149.8 40.1 all-gather.6
where the time goes:
time: 232 us
  waiting for transfers between devices  85.6 us (37%)
  blocking collectives  76.6 us (33%)
  local copies, waits for them, and re-layouts  34.6 us (15%)
  between operations  13.6 us (6%)
  starting transfers between devices  13.3 us (6%)
  matrix products  4.82 us (2%)
  other arithmetic  3.18 us (1%)
    all_gather x2, waiting for transfers between devices, whole_of(): nearer = lax.all_gather(shard, axes[-1], axis=dim, tiled=True)  69.7 us
    all_to_all x1, blocking collectives, body(): lax.all_to_all(outgoing, 'ep', split_axis=0, concat_axis=0, tiled=True)  35.8 us
    scatter x1, local copies, waits for them, and re-layouts, body(): slot_table = jnp.full((expert_total, capacity), tok_rows, jnp.int32).at[f...  25.1 us
    all_gather x2, blocking collectives, whole_of(): nearer = lax.all_gather(shard, axes[-1], axis=dim, tiled=True)  22.8 us
    psum x2, blocking collectives, by_axis(): shard = lax.psum(shard, axis)  18 us
    all_to_all x1, waiting for transfers between devices, body(): lax.all_to_all(sendback, 'ep', split_axis=0, concat_axis=0, tiled=True)  15.9 us
    all_to_all x1, starting transfers between devices, body(): lax.all_to_all(sendback, 'ep', split_axis=0, concat_axis=0, tiled=True)  13.3 us
  transfers between devices with their start and end apart: 3, of which 3 were waited for; matrix products, arithmetic and copies ran while one was open for 0% of the time, Pallas kernels for 0%

commit v1 on v0

v1 whole, which is shorter than its diff:
```python
import jax
import jax.numpy as jnp
from jax import lax
from jax.experimental import pallas as pl
from jax.experimental.pallas import tpu as pltpu
from jax.sharding import PartitionSpec as P

MESH = pl.DeviceIdType.MESH
F32 = jnp.float32
BF16 = jnp.bfloat16

EPSILON = 1e-06
ALPHA = 1.702
LIMIT = 7.0

NZ = 16
Q = 4
D = 1024
TOK = 128
EXPERTS = 32
TOPK = 4
HALF = 64
Z_ORDER = (8, 7, 9, 6, 10, 5, 11, 4, 12, 3, 13, 2, 14, 1, 15, 0)


def iota(shape, dim):
    return lax.broadcasted_iota(jnp.int32, shape, dim)


def dot(a, b):
    return jnp.dot(a, b, preferred_element_type=F32)


def placed(offset):
    return jnp.where(iota((HALF, 128), 1) == iota((HALF, 128), 0) + offset, 1.0, 0.0).astype(BF16)


def swap(a, b):
    low = iota(a.shape, 1) < HALF
    return jnp.where(low, a, pltpu.roll(b, HALF, 1)), jnp.where(low, pltpu.roll(a, HALF, 1), b)


def kernel(
    tok_hbm, gain_hbm, gate_hbm, up_hbm, down_hbm, ids_hbm, rw_hbm, out_ref,
    tok, gain, gate, up, down, ids, rw,
    pbuf, gub, dnb, dnf, xb, hb, ob, rb,
    in_sem, disp_send, disp_recv, ret_send, ret_recv, ring_send, ring_recv,
):
    ep = lax.axis_index("ep")
    tp = lax.axis_index("tp")
    z, c = ep // 2, ep % 2
    y, x = tp // Q, tp % Q
    x_right, x_left = (x + 1) % Q, (x + 3) % Q
    y_right, y_left = (y + 1) % Q, (y + 3) % Q

    loads = []
    for i, (src, dst) in enumerate(
        ((ids_hbm, ids), (tok_hbm, tok), (gate_hbm.at[0], gate), (up_hbm.at[0], up),
         (down_hbm.at[0], down), (gain_hbm, gain), (rw_hbm, rw))
    ):
        load = pltpu.make_async_copy(src, dst, in_sem.at[i])
        load.start()
        loads.append(load)

    barrier = pltpu.get_barrier_semaphore()

    def greet(device):
        pl.semaphore_signal(barrier, inc=1, device_id=device, device_id_type=MESH)

    for m in range(Q):
        z_from = (z - (m * Q + y) + NZ) % NZ
        for cs in range(2):
            for ys in range(Q):
                device = (z_from * 2 + cs, ys * Q + x)
                if m == 0 and ys == 0:
                    @pl.when(jnp.logical_not(jnp.logical_and(y == 0, c == cs)))
                    def _():
                        greet(device)
                else:
                    greet(device)
    greet((ep, y * Q + x_right))
    greet((ep, y * Q + x_left))
    greet((ep, y_right * Q + x))
    greet((ep, y_left * Q + x))

    loads[0].wait()
    experts = iota((TOK, EXPERTS), 1)
    named = [ids[:, k : k + 1] == experts for k in range(TOPK)]
    member = named[0] | named[1] | named[2] | named[3]
    member_f = jnp.where(member, 1.0, 0.0)
    lower = jnp.where(iota((TOK, TOK), 1) < iota((TOK, TOK), 0), 1.0, 0.0).astype(BF16)
    slot = dot(lower, member_f.astype(BF16))
    code = jnp.where(member, slot, -1.0).astype(BF16)
    expand = jnp.where(iota((EXPERTS, 512), 1) // 16 == iota((EXPERTS, 512), 0), 1.0, 0.0).astype(BF16)
    code_wide = dot(code, expand)
    place = (iota((TOK, 512), 1) % 16).astype(F32)
    pick_low = jnp.where(code_wide == place, 1.0, 0.0)
    pick_high = jnp.where(code_wide == place + 16.0, 1.0, 0.0)

    left_eye, right_eye = placed(0), placed(HALF)
    loads[1].wait()
    token_low = dot(tok[...], left_eye).astype(BF16)
    token_high = dot(tok[...], right_eye).astype(BF16)
    first = (((0,), (0,)), ((), ()))
    packed = lax.dot_general(
        pick_low.astype(BF16), token_low, first, preferred_element_type=F32
    ) + lax.dot_general(pick_high.astype(BF16), token_high, first, preferred_element_type=F32)
    pbuf[...] = packed.astype(BF16)

    loads[2].wait()
    loads[3].wait()
    gub[y] = (dot(gate[...], left_eye) + dot(up[...], right_eye)).astype(BF16)
    loads[4].wait()
    dnb[y] = (dot(down[0:512, :], left_eye) + dot(down[512:1024, :], right_eye)).astype(BF16)

    own_edge = jnp.where(y == 0, 1, 0)
    pl.semaphore_wait(barrier, 2 * NZ + 4 - own_edge)

    sends = []
    for dz in Z_ORDER:
        m, yd = dz // Q, dz % Q
        for ce in range(2):
            e = ((z + dz) % NZ) * 2 + ce
            copy = pltpu.make_async_remote_copy(
                src_ref=pbuf.at[pl.ds(pl.multiple_of(e * 16, 16), 16)],
                dst_ref=xb.at[x, y, pl.ds(pl.multiple_of((m * 2 + c) * 16, 16), 16)],
                send_sem=disp_send.at[dz * 2 + ce],
                recv_sem=disp_recv.at[(m * 2 + c) * Q + y],
                device_id=(e, yd * Q + x),
                device_id_type=MESH,
            )
            if dz == 0:
                own = jnp.logical_and(y == 0, c == ce)

                @pl.when(jnp.logical_not(own))
                def _():
                    copy.start()

                @pl.when(own)
                def _():
                    xb[x, 0, pl.ds(pl.multiple_of(c * 16, 16), 16), :] = pbuf[
                        pl.ds(pl.multiple_of(e * 16, 16), 16), :
                    ]
                sends.append((copy, own))
            else:
                copy.start()
                sends.append((copy, None))

    class Ring:
        def __init__(self, buf, half, mine, right, left, device, base):
            self.buf, self.half, self.mine, self.base = buf, half, mine, base
            self.right, self.left, self.device = right, left, device
            self.sent = []

        def part(self, owner, h):
            return self.buf.at[owner, pl.ds(h * self.half, self.half)]

        def copy(self, owner, h, to, index):
            return pltpu.make_async_remote_copy(
                src_ref=self.part(owner, h),
                dst_ref=self.part(owner, h),
                send_sem=ring_send.at[self.base + index],
                recv_sem=ring_recv.at[self.base + index],
                device_id=self.device(to),
                device_id_type=MESH,
            )

        def send(self, owner, h, to, index):
            copy = self.copy(owner, h, to, index)
            copy.start()
            self.sent.append(copy)

        def arrived(self, owner, h, index):
            self.copy(owner, h, self.right, index).wait_recv()

        def start(self):
            self.send(self.mine, 0, self.right, 0)
            self.send(self.mine, 1, self.left, 1)
            self.send(self.mine, 1, self.right, 2)
            self.send(self.mine, 0, self.left, 3)

        def forward(self):
            self.arrived(self.left, 0, 0)
            self.send(self.left, 0, self.right, 4)
            self.arrived(self.right, 1, 1)
            self.send(self.right, 1, self.left, 5)

        def finish(self):
            far = (self.mine + 2) % Q
            self.arrived(self.left, 1, 2)
            self.arrived(self.right, 0, 3)
            self.arrived(far, 0, 4)
            self.arrived(far, 1, 5)

        def drain(self):
            for copy in self.sent:
                copy.wait_send()

    def along_x(to):
        return (ep, y * Q + to)

    def along_y(to):
        return (ep, to * Q + x)

    gu_ring = Ring(gub, 512, y, y_right, y_left, along_y, 0)
    dn_ring = Ring(dnb, 256, y, y_right, y_left, along_y, 6)
    x_ring = Ring(xb, 2, x, x_right, x_left, along_x, 12)
    h_ring = Ring(hb, 1, x, x_right, x_left, along_x, 18)

    gu_ring.start()
    gu_ring.forward()
    dn_ring.start()

    def dispatch_arrived(m, cs, ys):
        pltpu.make_async_remote_copy(
            src_ref=pbuf.at[pl.ds(0, 16)],
            dst_ref=xb.at[x, ys, pl.ds((m * 2 + cs) * 16, 16)],
            send_sem=disp_send.at[0],
            recv_sem=disp_recv.at[(m * 2 + cs) * Q + ys],
            device_id=(ep, tp),
            device_id_type=MESH,
        ).wait_recv()

    for m in range(Q):
        for cs in range(2):
            for ys in range(Q):
                if m == 0 and ys == 0:
                    @pl.when(jnp.logical_not(jnp.logical_and(y == 0, c == cs)))
                    def _():
                        dispatch_arrived(m, cs, ys)
                else:
                    dispatch_arrived(m, cs, ys)

    x_ring.start()
    x_ring.forward()
    dn_ring.forward()
    x_ring.finish()

    loads[5].wait()
    loads[6].wait()
    groups = []
    square = jnp.zeros((256, 128), F32)
    for g in range(8):
        ys, xs = g // 2, (g % 2) * 2
        low, high = swap(xb[xs, ys].astype(F32), xb[xs + 1, ys].astype(F32))
        part = jnp.concatenate([low, high], axis=0)
        square = square + part * part
        groups.append(part)
    inverse = lax.rsqrt(jnp.sum(square, axis=1, keepdims=True) / D + EPSILON)
    rows = jnp.concatenate(
        [(groups[g] * inverse * gain[g : g + 1, :]).astype(BF16) for g in range(8)], axis=1
    )

    gu_ring.finish()
    for p in range(2):
        both = dot(rows, jnp.concatenate([gub[2 * p], gub[2 * p + 1]], axis=1))
        gate_pre, up_pre = swap(both[:, :128], both[:, 128:])
        gate_pre = jnp.minimum(gate_pre, LIMIT)
        up_pre = jnp.clip(up_pre, -LIMIT, LIMIT)
        hidden = (up_pre + 1.0) * gate_pre * jax.nn.sigmoid(ALPHA * gate_pre)
        hb[x, p] = hidden.astype(BF16)
    h_ring.start()
    h_ring.forward()

    dn_ring.finish()
    for n in range(2):
        low, high = swap(dnb[2 * n].astype(F32), dnb[2 * n + 1].astype(F32))
        for xs in range(Q):
            for p in range(2):
                for h in range(2):
                    src = (low, high)[p][HALF * (4 * h + xs) : HALF * (4 * h + xs) + HALF]
                    at = (xs * 2 + p) * 128 + h * HALF
                    dnf[at : at + HALF, n * 128 : n * 128 + 128] = src.astype(BF16)

    h_ring.finish()
    hidden_all = jnp.concatenate([hb[k // 2, k % 2] for k in range(8)], axis=1)
    result = dot(hidden_all, dnf[...])
    for n in range(2):
        cols = result[:, n * 128 : n * 128 + 128]
        ob[2 * n], ob[2 * n + 1] = [v.astype(BF16) for v in swap(cols[:128], cols[128:])]

    for m in (2, 1, 3, 0):
        z_to = (z - (m * Q + y) + NZ) % NZ
        for cs in range(2):
            for ys in range(Q):
                copy = pltpu.make_async_remote_copy(
                    src_ref=ob.at[ys, pl.ds((m * 2 + cs) * 16, 16)],
                    dst_ref=rb.at[pl.ds(pl.multiple_of(ep * 16, 16), 16)],
                    send_sem=ret_send.at[(m * 2 + cs) * Q + ys],
                    recv_sem=ret_recv.at[ep],
                    device_id=(z_to * 2 + cs, ys * Q + x),
                    device_id_type=MESH,
                )
                if m == 0 and ys == 0:
                    own = jnp.logical_and(y == 0, c == cs)

                    @pl.when(jnp.logical_not(own))
                    def _():
                        copy.start()

                    @pl.when(own)
                    def _():
                        rb[pl.ds(pl.multiple_of(ep * 16, 16), 16), :] = ob[
                            0, cs * 16 : cs * 16 + 16, :
                        ]
                    sends.append((copy, own))
                else:
                    copy.start()
                    sends.append((copy, None))

    weight = jnp.zeros((TOK, EXPERTS), F32)
    for k in range(TOPK):
        weight = weight + jnp.where(named[k], rw[:, k : k + 1], 0.0)
    stack = []
    for pick in (pick_low, pick_high):
        rest = weight
        for _ in range(3):
            piece = rest.astype(BF16)
            rest = rest - piece.astype(F32)
            stack.append((dot(piece, expand) * pick).astype(BF16))
    mixer = jnp.concatenate(stack, axis=0)

    for dz in range(NZ):
        for ce in range(2):
            e = ((z + dz) % NZ) * 2 + ce
            arrived = pltpu.make_async_remote_copy(
                src_ref=ob.at[0, pl.ds(0, 16)],
                dst_ref=rb.at[pl.ds(pl.multiple_of(e * 16, 16), 16)],
                send_sem=ret_send.at[0],
                recv_sem=ret_recv.at[e],
                device_id=(ep, tp),
                device_id_type=MESH,
            )
            if dz == 0:
                @pl.when(jnp.logical_not(jnp.logical_and(y == 0, c == ce)))
                def _():
                    arrived.wait_recv()
            else:
                arrived.wait_recv()

    mixed = dot(mixer, rb[...])
    from_low = mixed[0:128] + mixed[128:256] + mixed[256:384]
    from_high = mixed[384:512] + mixed[512:640] + mixed[640:768]
    combined = from_low + pltpu.roll(from_high, HALF, 1)
    out_ref[...] = combined[:, :HALF].astype(BF16)

    for copy, own in sends:
        if own is None:
            copy.wait_send()
        else:
            @pl.when(jnp.logical_not(own))
            def _():
                copy.wait_send()
    for ring in (gu_ring, dn_ring, x_ring, h_ring):
        ring.drain()


def body(tokens, norm_gain, gate_weight, up_weight, down_weight, expert_ids, route_weight):
    return pl.pallas_call(
        kernel,
        out_shape=jax.ShapeDtypeStruct((TOK, HALF), BF16),
        in_specs=[pl.BlockSpec(memory_space=pl.ANY)] * 7,
        out_specs=pl.BlockSpec(memory_space=pltpu.VMEM),
        scratch_shapes=[
            pltpu.VMEM((TOK, HALF), BF16),
            pltpu.VMEM((8, 128), F32),
            pltpu.VMEM((D, HALF), BF16),
            pltpu.VMEM((D, HALF), BF16),
            pltpu.VMEM((D, HALF), BF16),
            pltpu.VMEM((TOK, TOPK), jnp.int32),
            pltpu.VMEM((TOK, TOPK), F32),
            pltpu.VMEM((512, 128), BF16),
            pltpu.VMEM((Q, D, 128), BF16),
            pltpu.VMEM((Q, 512, 128), BF16),
            pltpu.VMEM((D, 256), BF16),
            pltpu.VMEM((Q, Q, 128, 128), BF16),
            pltpu.VMEM((Q, 2, 256, 128), BF16),
            pltpu.VMEM((Q, 128, 128), BF16),
            pltpu.VMEM((512, 128), BF16),
            pltpu.SemaphoreType.DMA((7,)),
            pltpu.SemaphoreType.DMA((32,)),
            pltpu.SemaphoreType.DMA((32,)),
            pltpu.SemaphoreType.DMA((32,)),
            pltpu.SemaphoreType.DMA((32,)),
            pltpu.SemaphoreType.DMA((24,)),
            pltpu.SemaphoreType.DMA((24,)),
        ],
        compiler_params=pltpu.CompilerParams(collective_id=0, has_side_effects=True),
    )(
        tokens, norm_gain.reshape(8, 128), gate_weight, up_weight, down_weight,
        expert_ids, route_weight,
    )


def solution(mesh):
    in_specs = (
        P("ep", "tp"),
        P(),
        P("ep", None, "tp"),
        P("ep", None, "tp"),
        P("ep", None, "tp"),
        P("ep", None),
        P("ep", None),
    )
    return jax.shard_map(body, mesh=mesh, in_specs=in_specs, out_specs=P("ep", "tp"), check_vma=False)
```

time: 232 us -> 68.4 us (0.29)
  waiting for transfers between devices: 85.6 us -> 0 us
  blocking collectives: 76.6 us -> 0 us
  Pallas kernels: 0 us -> 59.1 us
  local copies, waits for them, and re-layouts: 34.6 us -> 8.38 us
  between operations: 13.6 us -> 0.02 us
  starting transfers between devices: 13.3 us -> 0 us
  matrix products: 4.82 us -> 0 us
  other arithmetic: 3.18 us -> 0 us
    all_gather x2 -> x0, waiting for transfers between devices: 69.7 us -> none  [whole_of(): nearer = lax.all_gather(shard, axes[-1], axis=dim, tiled=True)]
    pallas_call x0 -> x1, Pallas kernels: none -> 59.1 us  [body(): pl.pallas_call(kernel, out_shape=jax.ShapeDtypeStruct((TOK, HALF), BF16),...]
    all_to_all x1 -> x0, blocking collectives: 35.8 us -> none  [body(): lax.all_to_all(outgoing, 'ep', split_axis=0, concat_axis=0, tiled=True)]
    scatter x1 -> x0, local copies, waits for them, and re-layouts: 25.1 us -> none  [body(): slot_table = jnp.full((expert_total, capacity), tok_rows, jnp.int32).at[f...]
    all_gather x2 -> x0, blocking collectives: 22.8 us -> none  [whole_of(): nearer = lax.all_gather(shard, axes[-1], axis=dim, tiled=True)]
    psum x2 -> x0, blocking collectives: 18 us -> none  [by_axis(): shard = lax.psum(shard, axis)]
    all_to_all x1 -> x0, waiting for transfers between devices: 15.9 us -> none  [body(): lax.all_to_all(sendback, 'ep', split_axis=0, concat_axis=0, tiled=True)]
    all_to_all x1 -> x0, starting transfers between devices: 13.3 us -> none  [body(): lax.all_to_all(sendback, 'ep', split_axis=0, concat_axis=0, tiled=True)]
  transfers between devices with their start and end apart: 3 -> 0, of which waited for: 3 -> 0; matrix products, arithmetic and copies ran while one was open for 0% -> 0% of each run, Pallas kernels for 0% -> 0%
where the time goes in v1:
time: 68.4 us; the launch traced here: 67.5 us
  Pallas kernels  59.1 us (86%)
  local copies, waits for them, and re-layouts  8.38 us (12%)
    pallas_call x1, Pallas kernels, body(): pl.pallas_call(kernel, out_shape=jax.ShapeDtypeStruct((TOK, HALF), BF16),...  59.1 us
    unnamed x12, local copies, waits for them, and re-layouts  6.93 us
    pallas_call x1, local copies, waits for them, and re-layouts, body(): pl.pallas_call(kernel, out_shape=jax.ShapeDtypeStruct((TOK, HALF), BF16),...  1.45 us

profile of v1, /device:TPU:1, one launch (start us, length us, event | category | flops | bytes accessed | tf_op | source)
XLA Modules:
  0.0 67.5 jit_solution(10733005756338198722)
XLA Ops:
  0.0 0.0 copy-start
  0.0 1.5 %copy.8.tok_hbm = bf16[128,64]{1,0:T(8,128)(2,1)} copy(bf16[128,64]{0,1:T(8,128)(2,1)} %param.7) | data formatting | bytes 32768 | tf_op args[0]
  1.5 1.4 %copy.12.ids_hbm = s32[128,4]{1,0:T(8,128)} copy(s32[128,4]{0,1:T(4,128)} %param.12) | data formatting | bytes 4096 | tf_op args[5]
  2.9 1.4 %copy.13.rw_hbm = f32[128,4]{1,0:T(8,128)} copy(f32[128,4]{0,1:T(4,128)} %param.13) | data formatting | bytes 4096 | tf_op args[6]
  4.3 0.0 copy-done
  4.3 0.0 copy-start.1
  4.3 0.8 %copy.9.gate_hbm = bf16[1,1024,64]{2,1,0:T(8,128)(2,1)} copy(bf16[1,1024,64]{1,2,0:T(8,128)(2,1)S(1)} %copy-done) | data formatting | bytes 262144 | tf_op args[2]
  5.1 0.1 copy-done.1
  5.2 0.0 copy-start.2
  5.2 0.8 %copy.10.up_hbm = bf16[1,1024,64]{2,1,0:T(8,128)(2,1)} copy(bf16[1,1024,64]{1,2,0:T(8,128)(2,1)S(1)} %copy-done.1) | data formatting | bytes 262144 | tf_op args[3]
  6.0 0.1 copy-done.2
  6.1 0.8 %copy.11.down_hbm = bf16[1,1024,64]{2,1,0:T(8,128)(2,1)} copy(bf16[1,1024,64]{1,2,0:T(8,128)(2,1)S(1)} %copy-done.2) | data formatting | bytes 262144 | tf_op args[4]
  6.9 59.1 %shard_map.73 = bf16[128,64]{1,0:T(8,128)(2,1)} custom-call(bf16[128,64]{1,0:T(8,128)(2,1)} %copy.8.tok_hbm, f32[8,128]{1,0:T(8,128)} %bitcast.1, bf16[1,1024,64]{2,1,0:T(8,128)(2,1)} %copy.9.gate_hbm, bf16[1,1024,64]{2,1,0:T(8,128)(2,1)} %copy.10.up_hbm, bf16[1,1024,64]{2,1,0:T(8,128)(2,1)} %copy.11.down_hbm, s32[128,4]{1,0:T(8,128)} %copy.12.ids_hbm, ...), custom_call_target="tpu_custom_call" | custom-call | tf_op jit(solution)/shard_map/pallas_call | solution.py:359
  66.0 1.4 %copy.14 = bf16[128,64]{0,1:T(8,128)(2,1)} copy(bf16[128,64]{1,0:T(8,128)(2,1)} %shard_map.73) | data formatting | bytes 32768 | tf_op jit(solution)/shard_map/pallas_call | solution.py:359
Async XLA Ops:
  0.0 4.3 %copy-start = (bf16[1,1024,64]{1,2,0:T(8,128)(2,1)S(1)}, bf16[1,1024,64]{1,2,0:T(8,128)(2,1)}, u32[]{:S(2)}) copy-start(bf16[1,1024,64]{1,2,0:T(8,128)(2,1)} %param.9) | copy-start | bytes 393220
  4.3 0.9 %copy-start.1 = (bf16[1,1024,64]{1,2,0:T(8,128)(2,1)S(1)}, bf16[1,1024,64]{1,2,0:T(8,128)(2,1)}, u32[]{:S(2)}) copy-start(bf16[1,1024,64]{1,2,0:T(8,128)(2,1)} %param.10) | copy-start | bytes 393220
  5.2 0.9 %copy-start.2 = (bf16[1,1024,64]{1,2,0:T(8,128)(2,1)S(1)}, bf16[1,1024,64]{1,2,0:T(8,128)(2,1)}, u32[]{:S(2)}) copy-start(bf16[1,1024,64]{1,2,0:T(8,128)(2,1)} %param.11) | copy-start | bytes 393220

commit v2 on v1

--- a/solution.py
+++ b/solution.py
@@ -31,6 +31,14 @@
     return jnp.dot(a, b, preferred_element_type=F32)
 
 
+def dot_rows(a, b):
+    return lax.dot_general(a, b, (((1,), (1,)), ((), ())), preferred_element_type=F32)
+
+
+def dot_columns(a, b):
+    return lax.dot_general(a, b, (((0,), (0,)), ((), ())), preferred_element_type=F32)
+
+
 def placed(offset):
     return jnp.where(iota((HALF, 128), 1) == iota((HALF, 128), 0) + offset, 1.0, 0.0).astype(BF16)
 
@@ -42,8 +50,8 @@
 
 def kernel(
     tok_hbm, gain_hbm, gate_hbm, up_hbm, down_hbm, ids_hbm, rw_hbm, out_ref,
-    tok, gain, gate, up, down, ids, rw,
-    pbuf, gub, dnb, dnf, xb, hb, ob, rb,
+    tok, gain, ids, rw,
+    pbuf, gub, dnb, dnf, xb, hb, ob, rb, mixer,
     in_sem, disp_send, disp_recv, ret_send, ret_recv, ring_send, ring_recv,
 ):
     ep = lax.axis_index("ep")
@@ -55,8 +63,9 @@
 
     loads = []
     for i, (src, dst) in enumerate(
-        ((ids_hbm, ids), (tok_hbm, tok), (gate_hbm.at[0], gate), (up_hbm.at[0], up),
-         (down_hbm.at[0], down), (gain_hbm, gain), (rw_hbm, rw))
+        ((ids_hbm, ids), (tok_hbm, tok), (gate_hbm.at[0], gub.at[y, pl.ds(0, HALF)]),
+         (up_hbm.at[0], gub.at[y, pl.ds(HALF, HALF)]), (down_hbm.at[0], dnb.at[y]),
+         (gain_hbm, gain), (rw_hbm, rw))
     ):
         load = pltpu.make_async_copy(src, dst, in_sem.at[i])
         load.start()
@@ -84,35 +93,37 @@
     greet((ep, y_left * Q + x))
 
     loads[0].wait()
-    experts = iota((TOK, EXPERTS), 1)
-    named = [ids[:, k : k + 1] == experts for k in range(TOPK)]
+    experts = iota((EXPERTS, TOK), 0)
+    named = [ids[k : k + 1, :] == experts for k in range(TOPK)]
     member = named[0] | named[1] | named[2] | named[3]
-    member_f = jnp.where(member, 1.0, 0.0)
-    lower = jnp.where(iota((TOK, TOK), 1) < iota((TOK, TOK), 0), 1.0, 0.0).astype(BF16)
-    slot = dot(lower, member_f.astype(BF16))
+    earlier = jnp.where(iota((TOK, TOK), 0) < iota((TOK, TOK), 1), 1.0, 0.0).astype(BF16)
+    slot = dot(jnp.where(member, 1.0, 0.0).astype(BF16), earlier)
     code = jnp.where(member, slot, -1.0).astype(BF16)
-    expand = jnp.where(iota((EXPERTS, 512), 1) // 16 == iota((EXPERTS, 512), 0), 1.0, 0.0).astype(BF16)
-    code_wide = dot(code, expand)
-    place = (iota((TOK, 512), 1) % 16).astype(F32)
+    expand = jnp.where(iota((512, EXPERTS), 0) // 16 == iota((512, EXPERTS), 1), 1.0, 0.0).astype(BF16)
+    code_wide = dot(expand, code)
+    place = (iota((512, TOK), 0) % 16).astype(F32)
     pick_low = jnp.where(code_wide == place, 1.0, 0.0)
     pick_high = jnp.where(code_wide == place + 16.0, 1.0, 0.0)
 
-    left_eye, right_eye = placed(0), placed(HALF)
     loads[1].wait()
-    token_low = dot(tok[...], left_eye).astype(BF16)
-    token_high = dot(tok[...], right_eye).astype(BF16)
-    first = (((0,), (0,)), ((), ()))
-    packed = lax.dot_general(
-        pick_low.astype(BF16), token_low, first, preferred_element_type=F32
-    ) + lax.dot_general(pick_high.astype(BF16), token_high, first, preferred_element_type=F32)
+    token_low = dot_columns(tok[...], placed(0)).astype(BF16)
+    token_high = dot_columns(tok[...], placed(HALF)).astype(BF16)
+    packed = dot(pick_low.astype(BF16), token_low) + dot(pick_high.astype(BF16), token_high)
     pbuf[...] = packed.astype(BF16)
 
-    loads[2].wait()
-    loads[3].wait()
-    gub[y] = (dot(gate[...], left_eye) + dot(up[...], right_eye)).astype(BF16)
-    loads[4].wait()
-    dnb[y] = (dot(down[0:512, :], left_eye) + dot(down[512:1024, :], right_eye)).astype(BF16)
-
+    loads[6].wait()
+    weight = jnp.zeros((EXPERTS, TOK), F32)
+    for k in range(TOPK):
+        weight = weight + jnp.where(named[k], rw[k : k + 1, :], 0.0)
+    for i in range(3):
+        piece = weight.astype(BF16)
+        weight = weight - piece.astype(F32)
+        wide = dot(expand, piece)
+        mixer[:, i * 128 : i * 128 + 128] = (wide * pick_low).astype(BF16)
+        mixer[:, 384 + i * 128 : 512 + i * 128] = (wide * pick_high).astype(BF16)
+
+    for load in loads[2:6]:
+        load.wait()
     own_edge = jnp.where(y == 0, 1, 0)
     pl.semaphore_wait(barrier, 2 * NZ + 4 - own_edge)
 
@@ -202,8 +213,8 @@
     def along_y(to):
         return (ep, to * Q + x)
 
-    gu_ring = Ring(gub, 512, y, y_right, y_left, along_y, 0)
-    dn_ring = Ring(dnb, 256, y, y_right, y_left, along_y, 6)
+    gu_ring = Ring(gub, 64, y, y_right, y_left, along_y, 0)
+    dn_ring = Ring(dnb, 32, y, y_right, y_left, along_y, 6)
     x_ring = Ring(xb, 2, x, x_right, x_left, along_x, 12)
     h_ring = Ring(hb, 1, x, x_right, x_left, along_x, 18)
 
@@ -236,8 +247,6 @@
     dn_ring.forward()
     x_ring.finish()
 
-    loads[5].wait()
-    loads[6].wait()
     groups = []
     square = jnp.zeros((256, 128), F32)
     for g in range(8):
@@ -253,7 +262,7 @@
 
     gu_ring.finish()
     for p in range(2):
-        both = dot(rows, jnp.concatenate([gub[2 * p], gub[2 * p + 1]], axis=1))
+        both = dot_rows(rows, jnp.concatenate([gub[2 * p], gub[2 * p + 1]], axis=0))
         gate_pre, up_pre = swap(both[:, :128], both[:, 128:])
         gate_pre = jnp.minimum(gate_pre, LIMIT)
         up_pre = jnp.clip(up_pre, -LIMIT, LIMIT)
@@ -263,18 +272,20 @@
     h_ring.forward()
 
     dn_ring.finish()
-    for n in range(2):
-        low, high = swap(dnb[2 * n].astype(F32), dnb[2 * n + 1].astype(F32))
-        for xs in range(Q):
-            for p in range(2):
-                for h in range(2):
-                    src = (low, high)[p][HALF * (4 * h + xs) : HALF * (4 * h + xs) + HALF]
-                    at = (xs * 2 + p) * 128 + h * HALF
-                    dnf[at : at + HALF, n * 128 : n * 128 + 128] = src.astype(BF16)
+    for n in range(Q):
+        for p in range(2):
+            for m in range(2):
+                g = (4 * p + m) * 128
+                even, odd = swap(
+                    dnb[n, :, g : g + 128].astype(F32), dnb[n, :, g + 256 : g + 384].astype(F32)
+                )
+                at = (4 * m + p) * 128
+                dnf[n * HALF : n * HALF + HALF, at : at + 128] = even.astype(BF16)
+                dnf[n * HALF : n * HALF + HALF, at + 256 : at + 384] = odd.astype(BF16)
 
     h_ring.finish()
     hidden_all = jnp.concatenate([hb[k // 2, k % 2] for k in range(8)], axis=1)
-    result = dot(hidden_all, dnf[...])
+    result = dot_rows(hidden_all, dnf[...])
     for n in range(2):
         cols = result[:, n * 128 : n * 128 + 128]
         ob[2 * n], ob[2 * n + 1] = [v.astype(BF16) for v in swap(cols[:128], cols[128:])]
@@ -307,18 +318,6 @@
                 else:
                     copy.start()
                     sends.append((copy, None))
-
-    weight = jnp.zeros((TOK, EXPERTS), F32)
-    for k in range(TOPK):
-        weight = weight + jnp.where(named[k], rw[:, k : k + 1], 0.0)
-    stack = []
-    for pick in (pick_low, pick_high):
-        rest = weight
-        for _ in range(3):
-            piece = rest.astype(BF16)
-            rest = rest - piece.astype(F32)
-            stack.append((dot(piece, expand) * pick).astype(BF16))
-    mixer = jnp.concatenate(stack, axis=0)
 
     for dz in range(NZ):
         for ce in range(2):
@@ -338,11 +337,12 @@
             else:
                 arrived.wait_recv()
 
-    mixed = dot(mixer, rb[...])
-    from_low = mixed[0:128] + mixed[128:256] + mixed[256:384]
-    from_high = mixed[384:512] + mixed[512:640] + mixed[640:768]
-    combined = from_low + pltpu.roll(from_high, HALF, 1)
-    out_ref[...] = combined[:, :HALF].astype(BF16)
+    mixed = dot_columns(rb[...], mixer[...])
+    combined = mixed[0:HALF, 0:128] + mixed[HALF:128, 384:512]
+    for i in range(1, 3):
+        combined = combined + mixed[0:HALF, i * 128 : i * 128 + 128]
+        combined = combined + mixed[HALF:128, 384 + i * 128 : 512 + i * 128]
+    out_ref[...] = combined.astype(BF16)
 
     for copy, own in sends:
         if own is None:
@@ -356,27 +356,26 @@
 
 
 def body(tokens, norm_gain, gate_weight, up_weight, down_weight, expert_ids, route_weight):
+    turned = (0, 2, 1)
     return pl.pallas_call(
         kernel,
-        out_shape=jax.ShapeDtypeStruct((TOK, HALF), BF16),
+        out_shape=jax.ShapeDtypeStruct((HALF, TOK), BF16),
         in_specs=[pl.BlockSpec(memory_space=pl.ANY)] * 7,
         out_specs=pl.BlockSpec(memory_space=pltpu.VMEM),
         scratch_shapes=[
-            pltpu.VMEM((TOK, HALF), BF16),
+            pltpu.VMEM((HALF, TOK), BF16),
             pltpu.VMEM((8, 128), F32),
-            pltpu.VMEM((D, HALF), BF16),
-            pltpu.VMEM((D, HALF), BF16),
-            pltpu.VMEM((D, HALF), BF16),
-            pltpu.VMEM((TOK, TOPK), jnp.int32),
-            pltpu.VMEM((TOK, TOPK), F32),
+            pltpu.VMEM((TOPK, TOK), jnp.int32),
+            pltpu.VMEM((TOPK, TOK), F32),
             pltpu.VMEM((512, 128), BF16),
-            pltpu.VMEM((Q, D, 128), BF16),
-            pltpu.VMEM((Q, 512, 128), BF16),
-            pltpu.VMEM((D, 256), BF16),
+            pltpu.VMEM((Q, 128, D), BF16),
+            pltpu.VMEM((Q, HALF, D), BF16),
+            pltpu.VMEM((256, D), BF16),
             pltpu.VMEM((Q, Q, 128, 128), BF16),
             pltpu.VMEM((Q, 2, 256, 128), BF16),
             pltpu.VMEM((Q, 128, 128), BF16),
             pltpu.VMEM((512, 128), BF16),
+            pltpu.VMEM((512, 768), BF16),
             pltpu.SemaphoreType.DMA((7,)),
             pltpu.SemaphoreType.DMA((32,)),
             pltpu.SemaphoreType.DMA((32,)),
@@ -387,9 +386,9 @@
         ],
         compiler_params=pltpu.CompilerParams(collective_id=0, has_side_effects=True),
     )(
-        tokens, norm_gain.reshape(8, 128), gate_weight, up_weight, down_weight,
-        expert_ids, route_weight,
-    )
+        tokens.T, norm_gain.reshape(8, 128), gate_weight.transpose(turned), up_weight.transpose(turned),
+        down_weight.transpose(turned), expert_ids.T, route_weight.T,
+    ).T
 
 
 def solution(mesh):

time: 68.4 us -> 58.9 us (0.86)
  local copies, waits for them, and re-layouts: 8.38 us -> 1.32 us
  Pallas kernels: 59.1 us -> 57.3 us
    unnamed x12 -> x1, local copies, waits for them, and re-layouts: 6.93 us -> 1.32 us
    pallas_call x1, Pallas kernels: 59.1 us -> 57.3 us  [body(): pl.pallas_call(kernel, out_shape=jax.ShapeDtypeStruct((HALF, TOK), BF16),...]
    pallas_call x1 -> x0, local copies, waits for them, and re-layouts: 1.45 us -> none  [body(): pl.pallas_call(kernel, out_shape=jax.ShapeDtypeStruct((TOK, HALF), BF16),...]
where the time goes in v2:
time: 58.9 us; the launch traced here: 58.6 us
  Pallas kernels  57.3 us (97%)
  local copies, waits for them, and re-layouts  1.32 us (2%)
    pallas_call x1, Pallas kernels, body(): pl.pallas_call(kernel, out_shape=jax.ShapeDtypeStruct((HALF, TOK), BF16),...  57.3 us
    unnamed x1, local copies, waits for them, and re-layouts  1.32 us

profile of v2, /device:TPU:1, one launch (start us, length us, event | category | flops | bytes accessed | tf_op | source)
XLA Modules:
  0.0 58.6 jit_solution(5447514967505945590)
XLA Ops:
  0.0 57.3 %shard_map.73 = bf16[64,128]{1,0:T(8,128)(2,1)} custom-call(bf16[64,128]{1,0:T(8,128)(2,1)} %bitcast.12, f32[8,128]{1,0:T(8,128)} %bitcast.13, bf16[1,64,1024]{2,1,0:T(8,128)(2,1)} %bitcast.8, bf16[1,64,1024]{2,1,0:T(8,128)(2,1)} %bitcast.9, bf16[1,64,1024]{2,1,0:T(8,128)(2,1)} %bitcast.10, s32[4,128]{1,0:T(4,128)} %bitcast.14, f32[4,128]{1,0:T(4,128)} %bitcast.15), custom_call_target="tpu_custom_call" | custom-call | tf_op jit(solution)/shard_map/pallas_call | solution.py:360
  57.3 1.3 %copy.9 = bf16[128,64]{0,1:T(8,128)(2,1)} copy(bf16[128,64]{0,1:T(8,128)(2,1)} %bitcast.11) | data formatting | bytes 32768

commit v3 on v2

v3 whole, which is shorter than its diff:
```python
import jax
import jax.numpy as jnp
from jax import lax
from jax.experimental import pallas as pl
from jax.experimental.pallas import tpu as pltpu
from jax.sharding import PartitionSpec as P

MESH = pl.DeviceIdType.MESH
F32 = jnp.float32
BF16 = jnp.bfloat16

EPSILON = 1e-06
ALPHA = 1.702
LIMIT = 7.0

NZ = 16
Q = 4
D = 1024
TOK = 128
EXPERTS = 32
TOPK = 4
HALF = 64
Z_ORDER = (8, 7, 9, 6, 10, 5, 11, 4, 12, 3, 13, 2, 14, 1, 15, 0)
PARTS = ((0, 3), (1, 2))
M_AT = {m: i for i, m in enumerate(m for part in PARTS for m in part)}
N_PART = len(PARTS)
PACKED = 128 // N_PART


def iota(shape, dim):
    return lax.broadcasted_iota(jnp.int32, shape, dim)


def dot(a, b):
    return jnp.dot(a, b, preferred_element_type=F32)


def dot_rows(a, b):
    return lax.dot_general(a, b, (((1,), (1,)), ((), ())), preferred_element_type=F32)


def dot_columns(a, b):
    return lax.dot_general(a, b, (((0,), (0,)), ((), ())), preferred_element_type=F32)


def placed(offset):
    return jnp.where(iota((HALF, 128), 1) == iota((HALF, 128), 0) + offset, 1.0, 0.0).astype(BF16)


def swap(a, b):
    low = iota(a.shape, 1) < HALF
    return jnp.where(low, a, pltpu.roll(b, HALF, 1)), jnp.where(low, pltpu.roll(a, HALF, 1), b)


def bits(v):
    return v // 2, ((v + 1) % Q) // 2


def gray(a, b):
    return 3 * a + b - 2 * a * b


def place(k, quarter, column):
    if isinstance(k, int):
        a, b = (quarter, column) if k == 0 else (column, quarter)
    else:
        a = quarter + k * (column - quarter)
        b = column + k * (quarter - column)
    return gray(a // 2, b // 2) * Q + gray(a % 2, b % 2)


def rows_at(m, core):
    return (M_AT[m] * 2 + core) * 16


def tile(start):
    return pl.ds(start if isinstance(start, int) else pl.multiple_of(start, 16), 16)


class Gather:
    def __init__(self, view, mine, device, sems, base):
        self.view, self.device, self.base = view, device, base
        self.send_sems, self.recv_sems = sems
        self.mine = mine
        self.right = mine + 1 - 2 * (mine % 2)
        self.left = mine + 2 - 4 * (mine // 2)
        self.far = 3 - mine
        self.sent = []

    def copy(self, owner, h, to, index):
        return pltpu.make_async_remote_copy(
            src_ref=self.view(owner, h),
            dst_ref=self.view(owner, h),
            send_sem=self.send_sems.at[self.base + index],
            recv_sem=self.recv_sems.at[self.base + index],
            device_id=self.device(to),
            device_id_type=MESH,
        )

    def send(self, owner, h, to, index):
        copy = self.copy(owner, h, to, index)
        copy.start()
        self.sent.append(copy)

    def arrived(self, owner, h, index):
        self.copy(owner, h, self.right, index).wait_recv()

    def start(self):
        self.send(self.mine, 0, self.right, 0)
        self.send(self.mine, 1, self.left, 1)
        self.send(self.mine, 1, self.right, 2)
        self.send(self.mine, 0, self.left, 3)

    def forward(self):
        self.arrived(self.right, 0, 0)
        self.send(self.right, 0, self.left, 5)
        self.arrived(self.left, 1, 1)
        self.send(self.left, 1, self.right, 4)

    def finish(self):
        self.arrived(self.right, 1, 2)
        self.arrived(self.left, 0, 3)
        self.arrived(self.far, 1, 4)
        self.arrived(self.far, 0, 5)

    def drain(self):
        for copy in self.sent:
            copy.wait_send()


def kernel(
    tok_hbm, gain_hbm, gate_hbm, up_hbm, down_hbm, ids_hbm, rw_hbm, out_ref,
    tok, gain, ids, rw,
    pbuf, gub, dnb, dnf, xb, hb, ob, rb, mixer,
    in_sem, disp_send, disp_recv, ret_send, ret_recv, ring_send, ring_recv,
):
    ep = lax.axis_index("ep")
    tp = lax.axis_index("tp")
    z, c = ep // 2, ep % 2
    (ay, by), (ax, bx) = bits(tp // Q), bits(tp % Q)
    side_a, side_b = ay * 2 + ax, by * 2 + bx
    quarter_of, column_of = (side_a, side_b), (side_b, side_a)
    quarter = side_a + c * (side_b - side_a)
    column = side_b + c * (side_a - side_b)

    barrier = pltpu.get_barrier_semaphore()

    def greet(device):
        pl.semaphore_signal(barrier, inc=1, device_id=device, device_id_type=MESH)

    def with_column(to):
        return (ep, place(c, to, column))

    def with_quarter(to):
        return (ep, place(c, quarter, to))

    for m in (2, 1, 3, 0):
        z_from = (z - (m * Q + quarter) + NZ) % NZ
        for cs in range(2):
            for qs in range(Q):
                device = (z_from * 2 + cs, place(c, qs, column))
                if m == 0 and qs == 0:
                    @pl.when(jnp.logical_not(jnp.logical_and(quarter == 0, c == cs)))
                    def _():
                        greet(device)
                else:
                    greet(device)

    loads = []
    for i, (src, dst) in enumerate(
        ((ids_hbm, ids), (tok_hbm, tok), (gate_hbm.at[0], gub.at[quarter, pl.ds(0, HALF)]),
         (up_hbm.at[0], gub.at[quarter, pl.ds(HALF, HALF)]), (down_hbm.at[0], dnb.at[quarter]),
         (gain_hbm, gain), (rw_hbm, rw))
    ):
        load = pltpu.make_async_copy(src, dst, in_sem.at[i])
        load.start()
        loads.append(load)

    sems = (ring_send, ring_recv)
    gu = Gather(lambda o, h: gub.at[o, pl.ds(h * HALF, HALF)], quarter, with_column, sems, 0)
    dn = Gather(lambda o, h: dnb.at[o, pl.ds(h * 32, 32)], quarter, with_column, sems, 6)
    x_parts, h_parts = [], []
    for i in range(N_PART):
        span = pl.ds(i * PACKED, PACKED)
        x_parts.append(Gather(
            lambda o, h, span=span: xb.at[o, pl.ds(h * 2, 2), span], column, with_quarter, sems, 12 + 12 * i
        ))
        h_parts.append(Gather(
            lambda o, h, i=i: hb.at[i, o, h], column, with_quarter, sems, 18 + 12 * i
        ))
    for gather in (gu, x_parts[0]):
        greet(gather.device(gather.right))
        greet(gather.device(gather.left))

    loads[0].wait()
    experts = iota((EXPERTS, TOK), 0)
    named = [ids[k : k + 1, :] == experts for k in range(TOPK)]
    member = named[0] | named[1] | named[2] | named[3]
    earlier = jnp.where(iota((TOK, TOK), 0) < iota((TOK, TOK), 1), 1.0, 0.0).astype(BF16)
    slot = dot(jnp.where(member, 1.0, 0.0).astype(BF16), earlier)
    code = jnp.where(member, slot, -1.0).astype(BF16)
    expand = jnp.where(iota((512, EXPERTS), 0) // 16 == iota((512, EXPERTS), 1), 1.0, 0.0).astype(BF16)
    code_wide = dot(expand, code)
    slot_of_row = (iota((512, TOK), 0) % 16).astype(F32)
    pick_low = jnp.where(code_wide == slot_of_row, 1.0, 0.0)
    pick_high = jnp.where(code_wide == slot_of_row + 16.0, 1.0, 0.0)

    loads[1].wait()
    token_low = dot_columns(tok[...], placed(0)).astype(BF16)
    token_high = dot_columns(tok[...], placed(HALF)).astype(BF16)
    packed = dot(pick_low.astype(BF16), token_low) + dot(pick_high.astype(BF16), token_high)
    pbuf[...] = packed.astype(BF16)

    pl.semaphore_wait(barrier, 2 * NZ + 4 - jnp.where(quarter == 0, 1, 0))

    sends = []
    for dz in Z_ORDER:
        m = dz // Q
        for ce in range(2):
            e = ((z + dz) % NZ) * 2 + ce
            copy = pltpu.make_async_remote_copy(
                src_ref=pbuf.at[tile(e * 16)],
                dst_ref=xb.at[column_of[ce], quarter_of[ce], tile(rows_at(m, c))],
                send_sem=disp_send.at[dz * 2 + ce],
                recv_sem=disp_recv.at[(m * 2 + c) * Q + quarter_of[ce]],
                device_id=(e, place(ce, dz % Q, column_of[ce])),
                device_id_type=MESH,
            )
            if dz == 0:
                own = jnp.logical_and(quarter == 0, c == ce)

                @pl.when(jnp.logical_not(own))
                def _():
                    copy.start()

                @pl.when(own)
                def _():
                    xb[column, 0, tile(rows_at(0, c)), :] = pbuf[tile(e * 16), :]
                sends.append((copy, own))
            else:
                copy.start()
                sends.append((copy, None))

    for load in loads[2:5]:
        load.wait()
    gu.start()
    dn.start()

    loads[5].wait()
    loads[6].wait()
    weight = jnp.zeros((EXPERTS, TOK), F32)
    for k in range(TOPK):
        weight = weight + jnp.where(named[k], rw[k : k + 1, :], 0.0)
    for i in range(3):
        piece = weight.astype(BF16)
        weight = weight - piece.astype(F32)
        wide = dot(expand, piece)
        mixer[:, i * 128 : i * 128 + 128] = (wide * pick_low).astype(BF16)
        mixer[:, 384 + i * 128 : 512 + i * 128] = (wide * pick_high).astype(BF16)

    gu.forward()

    def await_dispatch(part):
        for m in PARTS[part]:
            for cs in range(2):
                for qs in range(Q):
                    arrived = pltpu.make_async_remote_copy(
                        src_ref=pbuf.at[tile(0)],
                        dst_ref=xb.at[column, qs, tile(rows_at(m, cs))],
                        send_sem=disp_send.at[0],
                        recv_sem=disp_recv.at[(m * 2 + cs) * Q + qs],
                        device_id=(ep, tp),
                        device_id_type=MESH,
                    )
                    if m == 0 and qs == 0:
                        @pl.when(jnp.logical_not(jnp.logical_and(quarter == 0, c == cs)))
                        def _():
                            arrived.wait_recv()
                    else:
                        arrived.wait_recv()

    def slice_at(s, part):
        (ty, uy), (tx, ux) = bits(s // Q), bits(s % Q)
        t, u = ty * 2 + tx, uy * 2 + ux
        return xb[u + c * (t - u), t + c * (u - t), part * PACKED : (part + 1) * PACKED].astype(F32)

    def make_hidden(part):
        groups = []
        square = jnp.zeros((2 * PACKED, 128), F32)
        for g in range(8):
            low, high = swap(slice_at(2 * g, part), slice_at(2 * g + 1, part))
            both = jnp.concatenate([low, high], axis=0)
            square = square + both * both
            groups.append(both)
        inverse = lax.rsqrt(jnp.sum(square, axis=1, keepdims=True) / D + EPSILON)
        rows = jnp.concatenate(
            [(groups[g] * inverse * gain[g : g + 1, :]).astype(BF16) for g in range(8)], axis=1
        )
        for p in range(2):
            both = dot_rows(rows, jnp.concatenate([gub[2 * p], gub[2 * p + 1]], axis=0))
            gate_pre, up_pre = swap(both[:, :128], both[:, 128:])
            gate_pre = jnp.minimum(gate_pre, LIMIT)
            up_pre = jnp.clip(up_pre, -LIMIT, LIMIT)
            hidden = (up_pre + 1.0) * gate_pre * jax.nn.sigmoid(ALPHA * gate_pre)
            hb[part, column, p] = hidden.astype(BF16)

    def order_down(k):
        low = iota((HALF, 128), 1) < HALF
        for n in range(Q):
            for o in range(Q):
                for p in range(2):
                    sides = []
                    for h in range(2):
                        s = place(k, 2 * p + h, o)
                        v = dnb[n, :, s // 2 * 128 : s // 2 * 128 + 128].astype(F32)
                        sides.append(v if s % 2 == h else pltpu.roll(v, HALF, 1))
                    at = (o * 2 + p) * 128
                    dnf[n * HALF : n * HALF + HALF, at : at + 128] = jnp.where(low, *sides).astype(BF16)

    def make_result(part):
        hidden_all = jnp.concatenate([hb[part, k // 2, k % 2] for k in range(8)], axis=1)
        result = dot_rows(hidden_all, dnf[...])
        at = part * PACKED
        for n in range(2):
            cols = result[:, n * 128 : n * 128 + 128]
            pair = swap(cols[:PACKED], cols[PACKED:])
            ob[2 * n, at : at + PACKED], ob[2 * n + 1, at : at + PACKED] = [v.astype(BF16) for v in pair]

    def send_back(part):
        for m in PARTS[part]:
            z_to = (z - (m * Q + quarter) + NZ) % NZ
            for cs in range(2):
                for qs in range(Q):
                    copy = pltpu.make_async_remote_copy(
                        src_ref=ob.at[qs, tile(rows_at(m, cs))],
                        dst_ref=rb.at[tile(ep * 16)],
                        send_sem=ret_send.at[(m * 2 + cs) * Q + qs],
                        recv_sem=ret_recv.at[ep],
                        device_id=(z_to * 2 + cs, place(c, qs, column)),
                        device_id_type=MESH,
                    )
                    if m == 0 and qs == 0:
                        own = jnp.logical_and(quarter == 0, c == cs)

                        @pl.when(jnp.logical_not(own))
                        def _():
                            copy.start()

                        @pl.when(own)
                        def _():
                            rb[tile(ep * 16), :] = ob[0, tile(rows_at(0, cs)), :]
                        sends.append((copy, own))
                    else:
                        copy.start()
                        sends.append((copy, None))

    near, far = 0, 1
    await_dispatch(near)
    x_parts[near].start()
    dn.forward()
    x_parts[near].forward()
    x_parts[near].finish()
    gu.finish()
    make_hidden(near)
    h_parts[near].start()
    await_dispatch(far)
    x_parts[far].start()
    h_parts[near].forward()
    dn.finish()
    for k in range(2):
        @pl.when(c == k)
        def _():
            order_down(k)
    x_parts[far].forward()
    x_parts[far].finish()
    make_hidden(far)
    h_parts[far].start()
    h_parts[near].finish()
    make_result(near)
    send_back(near)
    h_parts[far].forward()
    h_parts[far].finish()
    make_result(far)
    send_back(far)

    for dz in range(NZ):
        for ce in range(2):
            e = ((z + dz) % NZ) * 2 + ce
            arrived = pltpu.make_async_remote_copy(
                src_ref=ob.at[0, tile(0)],
                dst_ref=rb.at[tile(e * 16)],
                send_sem=ret_send.at[0],
                recv_sem=ret_recv.at[e],
                device_id=(ep, tp),
                device_id_type=MESH,
            )
            if dz == 0:
                @pl.when(jnp.logical_not(jnp.logical_and(quarter_of[ce] == 0, c == ce)))
                def _():
                    arrived.wait_recv()
            else:
                arrived.wait_recv()

    mixed = dot_columns(rb[...], mixer[...])
    combined = mixed[0:HALF, 0:128] + mixed[HALF:128, 384:512]
    for i in range(1, 3):
        combined = combined + mixed[0:HALF, i * 128 : i * 128 + 128]
        combined = combined + mixed[HALF:128, 384 + i * 128 : 512 + i * 128]
    out_ref[...] = combined.astype(BF16)

    for copy, own in sends:
        if own is None:
            copy.wait_send()
        else:
            @pl.when(jnp.logical_not(own))
            def _():
                copy.wait_send()
    for gather in [gu, dn] + x_parts + h_parts:
        gather.drain()


def body(tokens, norm_gain, gate_weight, up_weight, down_weight, expert_ids, route_weight):
    turned = (0, 2, 1)
    return pl.pallas_call(
        kernel,
        out_shape=jax.ShapeDtypeStruct((HALF, TOK), BF16),
        in_specs=[pl.BlockSpec(memory_space=pl.ANY)] * 7,
        out_specs=pl.BlockSpec(memory_space=pltpu.VMEM),
        scratch_shapes=[
            pltpu.VMEM((HALF, TOK), BF16),
            pltpu.VMEM((8, 128), F32),
            pltpu.VMEM((TOPK, TOK), jnp.int32),
            pltpu.VMEM((TOPK, TOK), F32),
            pltpu.VMEM((512, 128), BF16),
            pltpu.VMEM((Q, 128, D), BF16),
            pltpu.VMEM((Q, HALF, D), BF16),
            pltpu.VMEM((256, D), BF16),
            pltpu.VMEM((Q, Q, 128, 128), BF16),
            pltpu.VMEM((N_PART, Q, 2, 2 * PACKED, 128), BF16),
            pltpu.VMEM((Q, 128, 128), BF16),
            pltpu.VMEM((512, 128), BF16),
            pltpu.VMEM((512, 768), BF16),
            pltpu.SemaphoreType.DMA((7,)),
            pltpu.SemaphoreType.DMA((32,)),
            pltpu.SemaphoreType.DMA((32,)),
            pltpu.SemaphoreType.DMA((32,)),
            pltpu.SemaphoreType.DMA((32,)),
            pltpu.SemaphoreType.DMA((12 + 12 * N_PART,)),
            pltpu.SemaphoreType.DMA((12 + 12 * N_PART,)),
        ],
        compiler_params=pltpu.CompilerParams(collective_id=0, has_side_effects=True),
    )(
        tokens.T, norm_gain.reshape(8, 128), gate_weight.transpose(turned), up_weight.transpose(turned),
        down_weight.transpose(turned), expert_ids.T, route_weight.T,
    ).T


def solution(mesh):
    in_specs = (
        P("ep", "tp"),
        P(),
        P("ep", None, "tp"),
        P("ep", None, "tp"),
        P("ep", None, "tp"),
        P("ep", None),
        P("ep", None),
    )
    return jax.shard_map(body, mesh=mesh, in_specs=in_specs, out_specs=P("ep", "tp"), check_vma=False)
```

time: 58.9 us -> 65.8 us (1.12)
  Pallas kernels: 57.3 us -> 64.2 us
    pallas_call x1, Pallas kernels: 57.3 us -> 64.2 us  [body(): pl.pallas_call(kernel, out_shape=jax.ShapeDtypeStruct((HALF, TOK), BF16),...]
where the time goes in v3:
time: 65.8 us; the launch traced here: 65.6 us
  Pallas kernels  64.2 us (98%)
  local copies, waits for them, and re-layouts  1.32 us (2%)
    pallas_call x1, Pallas kernels, body(): pl.pallas_call(kernel, out_shape=jax.ShapeDtypeStruct((HALF, TOK), BF16),...  64.2 us
    unnamed x1, local copies, waits for them, and re-layouts  1.32 us

profile of v3, /device:TPU:1, one launch (start us, length us, event | category | flops | bytes accessed | tf_op | source)
XLA Modules:
  0.0 65.6 jit_solution(16264274763208700303)
XLA Ops:
  0.0 64.2 %shard_map.73 = bf16[64,128]{1,0:T(8,128)(2,1)} custom-call(bf16[64,128]{1,0:T(8,128)(2,1)} %bitcast.12, f32[8,128]{1,0:T(8,128)} %bitcast.13, bf16[1,64,1024]{2,1,0:T(8,128)(2,1)} %bitcast.8, bf16[1,64,1024]{2,1,0:T(8,128)(2,1)} %bitcast.9, bf16[1,64,1024]{2,1,0:T(8,128)(2,1)} %bitcast.10, s32[4,128]{1,0:T(4,128)} %bitcast.14, f32[4,128]{1,0:T(4,128)} %bitcast.15), custom_call_target="tpu_custom_call" | custom-call | tf_op jit(solution)/shard_map/pallas_call | solution.py:424
  64.2 1.3 %copy.9 = bf16[128,64]{0,1:T(8,128)(2,1)} copy(bf16[128,64]{0,1:T(8,128)(2,1)} %bitcast.11) | data formatting | bytes 32768

commit v4 on v3

--- a/solution.py
+++ b/solution.py
@@ -21,7 +21,7 @@
 TOPK = 4
 HALF = 64
 Z_ORDER = (8, 7, 9, 6, 10, 5, 11, 4, 12, 3, 13, 2, 14, 1, 15, 0)
-PARTS = ((0, 3), (1, 2))
+PARTS = ((2, 1), (3, 0))
 M_AT = {m: i for i, m in enumerate(m for part in PARTS for m in part)}
 N_PART = len(PARTS)
 PACKED = 128 // N_PART
@@ -78,7 +78,8 @@
 
 
 class Gather:
-    def __init__(self, view, mine, device, sems, base):
+    def __init__(self, view, mine, device, sems, base, direct=False):
+        self.direct = direct
         self.view, self.device, self.base = view, device, base
         self.send_sems, self.recv_sems = sems
         self.mine = mine
@@ -110,6 +111,9 @@
         self.send(self.mine, 1, self.left, 1)
         self.send(self.mine, 1, self.right, 2)
         self.send(self.mine, 0, self.left, 3)
+        if self.direct:
+            self.send(self.mine, 1, self.far, 4)
+            self.send(self.mine, 0, self.far, 5)
 
     def forward(self):
         self.arrived(self.right, 0, 0)
@@ -118,6 +122,9 @@
         self.send(self.left, 1, self.right, 4)
 
     def finish(self):
+        if self.direct:
+            self.arrived(self.right, 0, 0)
+            self.arrived(self.left, 1, 1)
         self.arrived(self.right, 1, 2)
         self.arrived(self.left, 0, 3)
         self.arrived(self.far, 1, 4)
@@ -143,6 +150,16 @@
     quarter = side_a + c * (side_b - side_a)
     column = side_b + c * (side_a - side_b)
 
+    loads = []
+    for i, (src, dst) in enumerate(
+        ((ids_hbm, ids), (tok_hbm, tok), (gate_hbm.at[0], gub.at[quarter, pl.ds(0, HALF)]),
+         (up_hbm.at[0], gub.at[quarter, pl.ds(HALF, HALF)]), (down_hbm.at[0], dnb.at[quarter]),
+         (gain_hbm, gain), (rw_hbm, rw))
+    ):
+        load = pltpu.make_async_copy(src, dst, in_sem.at[i])
+        load.start()
+        loads.append(load)
+
     barrier = pltpu.get_barrier_semaphore()
 
     def greet(device):
@@ -166,16 +183,6 @@
                 else:
                     greet(device)
 
-    loads = []
-    for i, (src, dst) in enumerate(
-        ((ids_hbm, ids), (tok_hbm, tok), (gate_hbm.at[0], gub.at[quarter, pl.ds(0, HALF)]),
-         (up_hbm.at[0], gub.at[quarter, pl.ds(HALF, HALF)]), (down_hbm.at[0], dnb.at[quarter]),
-         (gain_hbm, gain), (rw_hbm, rw))
-    ):
-        load = pltpu.make_async_copy(src, dst, in_sem.at[i])
-        load.start()
-        loads.append(load)
-
     sems = (ring_send, ring_recv)
     gu = Gather(lambda o, h: gub.at[o, pl.ds(h * HALF, HALF)], quarter, with_column, sems, 0)
     dn = Gather(lambda o, h: dnb.at[o, pl.ds(h * 32, 32)], quarter, with_column, sems, 6)
@@ -183,14 +190,15 @@
     for i in range(N_PART):
         span = pl.ds(i * PACKED, PACKED)
         x_parts.append(Gather(
-            lambda o, h, span=span: xb.at[o, pl.ds(h * 2, 2), span], column, with_quarter, sems, 12 + 12 * i
+            lambda o, h, span=span: xb.at[o, pl.ds(h * 2, 2), span], column, with_quarter, sems, 12 + 12 * i, True
         ))
         h_parts.append(Gather(
-            lambda o, h, i=i: hb.at[i, o, h], column, with_quarter, sems, 18 + 12 * i
+            lambda o, h, i=i: hb.at[i, o, h], column, with_quarter, sems, 18 + 12 * i, True
         ))
     for gather in (gu, x_parts[0]):
         greet(gather.device(gather.right))
         greet(gather.device(gather.left))
+    greet(x_parts[0].device(x_parts[0].far))
 
     loads[0].wait()
     experts = iota((EXPERTS, TOK), 0)
@@ -211,7 +219,7 @@
     packed = dot(pick_low.astype(BF16), token_low) + dot(pick_high.astype(BF16), token_high)
     pbuf[...] = packed.astype(BF16)
 
-    pl.semaphore_wait(barrier, 2 * NZ + 4 - jnp.where(quarter == 0, 1, 0))
+    pl.semaphore_wait(barrier, 2 * NZ + 5 - jnp.where(quarter == 0, 1, 0))
 
     sends = []
     for dz in Z_ORDER:
@@ -259,6 +267,7 @@
         mixer[:, 384 + i * 128 : 512 + i * 128] = (wide * pick_high).astype(BF16)
 
     gu.forward()
+    dn.forward()
 
     def await_dispatch(part):
         for m in PARTS[part]:
@@ -354,34 +363,29 @@
                         copy.start()
                         sends.append((copy, None))
 
-    near, far = 0, 1
+    far, near = 0, 1
+    await_dispatch(far)
+    x_parts[far].start()
     await_dispatch(near)
     x_parts[near].start()
-    dn.forward()
-    x_parts[near].forward()
-    x_parts[near].finish()
+    x_parts[far].finish()
     gu.finish()
-    make_hidden(near)
-    h_parts[near].start()
-    await_dispatch(far)
-    x_parts[far].start()
-    h_parts[near].forward()
+    make_hidden(far)
+    h_parts[far].start()
     dn.finish()
     for k in range(2):
         @pl.when(c == k)
         def _():
             order_down(k)
-    x_parts[far].forward()
-    x_parts[far].finish()
-    make_hidden(far)
-    h_parts[far].start()
+    x_parts[near].finish()
+    make_hidden(near)
+    h_parts[near].start()
+    h_parts[far].finish()
+    make_result(far)
+    send_back(far)
     h_parts[near].finish()
     make_result(near)
     send_back(near)
-    h_parts[far].forward()
-    h_parts[far].finish()
-    make_result(far)
-    send_back(far)
 
     for dz in range(NZ):
         for ce in range(2):

time: 65.8 us -> 55.7 us (0.85)
  Pallas kernels: 64.2 us -> 54.2 us
    pallas_call x1, Pallas kernels: 64.2 us -> 54.2 us  [body(): pl.pallas_call(kernel, out_shape=jax.ShapeDtypeStruct((HALF, TOK), BF16),...]
where the time goes in v4:
time: 55.7 us; the launch traced here: 55.5 us
  Pallas kernels  54.2 us (97%)
  local copies, waits for them, and re-layouts  1.32 us (2%)
    pallas_call x1, Pallas kernels, body(): pl.pallas_call(kernel, out_shape=jax.ShapeDtypeStruct((HALF, TOK), BF16),...  54.2 us
    unnamed x1, local copies, waits for them, and re-layouts  1.32 us

profile of v4, /device:TPU:1, one launch (start us, length us, event | category | flops | bytes accessed | tf_op | source)
XLA Modules:
  0.0 55.5 jit_solution(3888330208055241127)
XLA Ops:
  0.0 54.2 %shard_map.73 = bf16[64,128]{1,0:T(8,128)(2,1)} custom-call(bf16[64,128]{1,0:T(8,128)(2,1)} %bitcast.12, f32[8,128]{1,0:T(8,128)} %bitcast.13, bf16[1,64,1024]{2,1,0:T(8,128)(2,1)} %bitcast.8, bf16[1,64,1024]{2,1,0:T(8,128)(2,1)} %bitcast.9, bf16[1,64,1024]{2,1,0:T(8,128)(2,1)} %bitcast.10, s32[4,128]{1,0:T(4,128)} %bitcast.14, f32[4,128]{1,0:T(4,128)} %bitcast.15), custom_call_target="tpu_custom_call" | custom-call | tf_op jit(solution)/shard_map/pallas_call | solution.py:428
  54.2 1.3 %copy.9 = bf16[128,64]{0,1:T(8,128)(2,1)} copy(bf16[128,64]{0,1:T(8,128)(2,1)} %bitcast.11) | data formatting | bytes 32768

commit v5 on v4

--- a/solution.py
+++ b/solution.py
@@ -21,10 +21,8 @@
 TOPK = 4
 HALF = 64
 Z_ORDER = (8, 7, 9, 6, 10, 5, 11, 4, 12, 3, 13, 2, 14, 1, 15, 0)
-PARTS = ((2, 1), (3, 0))
-M_AT = {m: i for i, m in enumerate(m for part in PARTS for m in part)}
+PARTS = ((0,), (1,), (2, 3))
 N_PART = len(PARTS)
-PACKED = 128 // N_PART
 
 
 def iota(shape, dim):
@@ -62,15 +60,15 @@
 
 def place(k, quarter, column):
     if isinstance(k, int):
-        a, b = (quarter, column) if k == 0 else (column, quarter)
+        a, b = (column, quarter) if k == 0 else (quarter, column)
     else:
-        a = quarter + k * (column - quarter)
-        b = column + k * (quarter - column)
+        a = column + k * (quarter - column)
+        b = quarter + k * (column - quarter)
     return gray(a // 2, b // 2) * Q + gray(a % 2, b % 2)
 
 
-def rows_at(m, core):
-    return (M_AT[m] * 2 + core) * 16
+def rows_at(j, core):
+    return (j * 2 + core) * 16
 
 
 def tile(start):
@@ -78,8 +76,7 @@
 
 
 class Gather:
-    def __init__(self, view, mine, device, sems, base, direct=False):
-        self.direct = direct
+    def __init__(self, view, mine, device, sems, base):
         self.view, self.device, self.base = view, device, base
         self.send_sems, self.recv_sems = sems
         self.mine = mine
@@ -111,9 +108,6 @@
         self.send(self.mine, 1, self.left, 1)
         self.send(self.mine, 1, self.right, 2)
         self.send(self.mine, 0, self.left, 3)
-        if self.direct:
-            self.send(self.mine, 1, self.far, 4)
-            self.send(self.mine, 0, self.far, 5)
 
     def forward(self):
         self.arrived(self.right, 0, 0)
@@ -122,13 +116,51 @@
         self.send(self.left, 1, self.right, 4)
 
     def finish(self):
-        if self.direct:
-            self.arrived(self.right, 0, 0)
-            self.arrived(self.left, 1, 1)
         self.arrived(self.right, 1, 2)
         self.arrived(self.left, 0, 3)
         self.arrived(self.far, 1, 4)
         self.arrived(self.far, 0, 5)
+
+    def drain(self):
+        for copy in self.sent:
+            copy.wait_send()
+
+
+class Exchange:
+    def __init__(self, view, pieces, mine, device, sems, base):
+        self.view, self.device, self.base = view, device, base
+        self.pieces = pieces
+        self.send_sems, self.recv_sems = sems
+        self.mine = mine
+        self.right = mine + 1 - 2 * (mine % 2)
+        self.left = mine + 2 - 4 * (mine // 2)
+        self.far = 3 - mine
+        self.others = (self.far, self.right, self.left)
+        self.sent = []
+
+    def copy(self, owner, h, to, index):
+        return pltpu.make_async_remote_copy(
+            src_ref=self.view(owner, h),
+            dst_ref=self.view(owner, h),
+            send_sem=self.send_sems.at[self.base + 3 * h + index],
+            recv_sem=self.recv_sems.at[self.base + 3 * h + index],
+            device_id=self.device(to),
+            device_id_type=MESH,
+        )
+
+    def send(self, h):
+        for index, to in enumerate(self.others):
+            copy = self.copy(self.mine, h, to, index)
+            copy.start()
+            self.sent.append(copy)
+
+    def arrived(self, index):
+        for h in range(self.pieces):
+            self.copy(self.others[index], h, self.right, index).wait_recv()
+
+    def finish(self):
+        for index in (1, 2, 0):
+            self.arrived(index)
 
     def drain(self):
         for copy in self.sent:
@@ -146,9 +178,9 @@
     z, c = ep // 2, ep % 2
     (ay, by), (ax, bx) = bits(tp // Q), bits(tp % Q)
     side_a, side_b = ay * 2 + ax, by * 2 + bx
-    quarter_of, column_of = (side_a, side_b), (side_b, side_a)
-    quarter = side_a + c * (side_b - side_a)
-    column = side_b + c * (side_a - side_b)
+    quarter_of, column_of = (side_b, side_a), (side_a, side_b)
+    quarter = side_b + c * (side_a - side_b)
+    column = side_a + c * (side_b - side_a)
 
     loads = []
     for i, (src, dst) in enumerate(
@@ -171,13 +203,18 @@
     def with_quarter(to):
         return (ep, place(c, quarter, to))
 
-    for m in (2, 1, 3, 0):
-        z_from = (z - (m * Q + quarter) + NZ) % NZ
+    z_low = (z - quarter + NZ) % Q
+
+    def is_own(j, cs):
+        return jnp.logical_and(jnp.logical_and(quarter == 0, c == cs), z // Q == j)
+
+    for j in range(Q):
+        z_from = j * Q + z_low
         for cs in range(2):
             for qs in range(Q):
                 device = (z_from * 2 + cs, place(c, qs, column))
-                if m == 0 and qs == 0:
-                    @pl.when(jnp.logical_not(jnp.logical_and(quarter == 0, c == cs)))
+                if qs == 0:
+                    @pl.when(jnp.logical_not(is_own(j, cs)))
                     def _():
                         greet(device)
                 else:
@@ -187,13 +224,14 @@
     gu = Gather(lambda o, h: gub.at[o, pl.ds(h * HALF, HALF)], quarter, with_column, sems, 0)
     dn = Gather(lambda o, h: dnb.at[o, pl.ds(h * 32, 32)], quarter, with_column, sems, 6)
     x_parts, h_parts = [], []
-    for i in range(N_PART):
-        span = pl.ds(i * PACKED, PACKED)
-        x_parts.append(Gather(
-            lambda o, h, span=span: xb.at[o, pl.ds(h * 2, 2), span], column, with_quarter, sems, 12 + 12 * i, True
+    for i, part in enumerate(PARTS):
+        x_parts.append(Exchange(
+            lambda o, h, first=part[0]: xb.at[o, :, pl.ds((first + h) * 32, 32)],
+            len(part), column, with_quarter, sems, 12 + 12 * i,
         ))
-        h_parts.append(Gather(
-            lambda o, h, i=i: hb.at[i, o, h], column, with_quarter, sems, 18 + 12 * i, True
+        h_parts.append(Exchange(
+            lambda o, h, part=part: hb.at[o, h, pl.ds(part[0] * 64, len(part) * 64)],
+            2, column, with_quarter, sems, 18 + 12 * i,
         ))
     for gather in (gu, x_parts[0]):
         greet(gather.device(gather.right))
@@ -221,33 +259,45 @@
 
     pl.semaphore_wait(barrier, 2 * NZ + 5 - jnp.where(quarter == 0, 1, 0))
 
+    def is_mine(dz, ce):
+        return jnp.logical_and(quarter == 0, c == ce) if dz == 0 else None
+
+    def dispatch():
+        for dz in Z_ORDER:
+            for ce in range(2):
+                e = ((z + dz) % NZ) * 2 + ce
+                copy = pltpu.make_async_remote_copy(
+                    src_ref=pbuf.at[tile(e * 16)],
+                    dst_ref=xb.at[column_of[ce], quarter_of[ce], tile(rows_at(z // Q, c))],
+                    send_sem=disp_send.at[dz * 2 + ce],
+                    recv_sem=disp_recv.at[(z // Q * 2 + c) * Q + quarter_of[ce]],
+                    device_id=(e, place(ce, dz % Q, column_of[ce])),
+                    device_id_type=MESH,
+                )
+                if dz == 0:
+                    @pl.when(jnp.logical_not(is_mine(dz, ce)))
+                    def _():
+                        copy.start()
+
+                    @pl.when(is_mine(dz, ce))
+                    def _():
+                        xb[column, 0, tile(rows_at(z // Q, c)), :] = pbuf[tile(e * 16), :]
+                else:
+                    copy.start()
+
     sends = []
     for dz in Z_ORDER:
-        m = dz // Q
         for ce in range(2):
-            e = ((z + dz) % NZ) * 2 + ce
-            copy = pltpu.make_async_remote_copy(
-                src_ref=pbuf.at[tile(e * 16)],
-                dst_ref=xb.at[column_of[ce], quarter_of[ce], tile(rows_at(m, c))],
+            sends.append((pltpu.make_async_remote_copy(
+                src_ref=pbuf.at[tile(0)],
+                dst_ref=pbuf.at[tile(0)],
                 send_sem=disp_send.at[dz * 2 + ce],
-                recv_sem=disp_recv.at[(m * 2 + c) * Q + quarter_of[ce]],
-                device_id=(e, place(ce, dz % Q, column_of[ce])),
+                recv_sem=disp_recv.at[0],
+                device_id=(ep, tp),
                 device_id_type=MESH,
-            )
-            if dz == 0:
-                own = jnp.logical_and(quarter == 0, c == ce)
-
-                @pl.when(jnp.logical_not(own))
-                def _():
-                    copy.start()
-
-                @pl.when(own)
-                def _():
-                    xb[column, 0, tile(rows_at(0, c)), :] = pbuf[tile(e * 16), :]
-                sends.append((copy, own))
-            else:
-                copy.start()
-                sends.append((copy, None))
+            ), is_mine(dz, ce)))
+
+    dispatch()
 
     for load in loads[2:5]:
         load.wait()
@@ -269,33 +319,36 @@
     gu.forward()
     dn.forward()
 
-    def await_dispatch(part):
-        for m in PARTS[part]:
+    def pass_rows(part):
+        for h, j in enumerate(PARTS[part]):
             for cs in range(2):
                 for qs in range(Q):
                     arrived = pltpu.make_async_remote_copy(
                         src_ref=pbuf.at[tile(0)],
-                        dst_ref=xb.at[column, qs, tile(rows_at(m, cs))],
+                        dst_ref=xb.at[column, qs, tile(rows_at(j, cs))],
                         send_sem=disp_send.at[0],
-                        recv_sem=disp_recv.at[(m * 2 + cs) * Q + qs],
+                        recv_sem=disp_recv.at[(j * 2 + cs) * Q + qs],
                         device_id=(ep, tp),
                         device_id_type=MESH,
                     )
-                    if m == 0 and qs == 0:
-                        @pl.when(jnp.logical_not(jnp.logical_and(quarter == 0, c == cs)))
+                    if qs == 0:
+                        @pl.when(jnp.logical_not(is_own(j, cs)))
                         def _():
                             arrived.wait_recv()
                     else:
                         arrived.wait_recv()
+            x_parts[part].send(h)
 
     def slice_at(s, part):
         (ty, uy), (tx, ux) = bits(s // Q), bits(s % Q)
         t, u = ty * 2 + tx, uy * 2 + ux
-        return xb[u + c * (t - u), t + c * (u - t), part * PACKED : (part + 1) * PACKED].astype(F32)
+        first, last = PARTS[part][0] * 32, PARTS[part][-1] * 32 + 32
+        return xb[t + c * (u - t), u + c * (t - u), first:last].astype(F32)
 
     def make_hidden(part):
         groups = []
-        square = jnp.zeros((2 * PACKED, 128), F32)
+        at, count = PARTS[part][0] * 64, len(PARTS[part]) * 64
+        square = jnp.zeros((count, 128), F32)
         for g in range(8):
             low, high = swap(slice_at(2 * g, part), slice_at(2 * g + 1, part))
             both = jnp.concatenate([low, high], axis=0)
@@ -311,7 +364,8 @@
             gate_pre = jnp.minimum(gate_pre, LIMIT)
             up_pre = jnp.clip(up_pre, -LIMIT, LIMIT)
             hidden = (up_pre + 1.0) * gate_pre * jax.nn.sigmoid(ALPHA * gate_pre)
-            hb[part, column, p] = hidden.astype(BF16)
+            hb[column, p, at : at + count] = hidden.astype(BF16)
+            h_parts[part].send(p)
 
     def order_down(k):
         low = iota((HALF, 128), 1) < HALF
@@ -323,33 +377,41 @@
                         s = place(k, 2 * p + h, o)
                         v = dnb[n, :, s // 2 * 128 : s // 2 * 128 + 128].astype(F32)
                         sides.append(v if s % 2 == h else pltpu.roll(v, HALF, 1))
-                    at = (o * 2 + p) * 128
-                    dnf[n * HALF : n * HALF + HALF, at : at + 128] = jnp.where(low, *sides).astype(BF16)
+                    dnf[o, n * HALF : n * HALF + HALF, p * 128 : p * 128 + 128] = jnp.where(low, *sides).astype(BF16)
 
     def make_result(part):
-        hidden_all = jnp.concatenate([hb[part, k // 2, k % 2] for k in range(8)], axis=1)
-        result = dot_rows(hidden_all, dnf[...])
-        at = part * PACKED
+        exchange = h_parts[part]
+        at, count = PARTS[part][0] * 32, len(PARTS[part]) * 32
+
+        def term(owner):
+            units = jnp.concatenate([hb[owner, p, 2 * at : 2 * at + 2 * count] for p in range(2)], axis=1)
+            return dot_rows(units, dnf[owner])
+
+        result = term(column)
+        for index in (1, 2, 0):
+            exchange.arrived(index)
+            result = result + term(exchange.others[index])
         for n in range(2):
             cols = result[:, n * 128 : n * 128 + 128]
-            pair = swap(cols[:PACKED], cols[PACKED:])
-            ob[2 * n, at : at + PACKED], ob[2 * n + 1, at : at + PACKED] = [v.astype(BF16) for v in pair]
-
-    def send_back(part):
-        for m in PARTS[part]:
-            z_to = (z - (m * Q + quarter) + NZ) % NZ
+            pair = swap(cols[:count], cols[count:])
+            ob[2 * n, at : at + count], ob[2 * n + 1, at : at + count] = [v.astype(BF16) for v in pair]
+            send_back(part, (2 * n, 2 * n + 1))
+
+    def send_back(part, quarters):
+        for j in PARTS[part]:
+            z_to = j * Q + z_low
             for cs in range(2):
-                for qs in range(Q):
+                for qs in quarters:
                     copy = pltpu.make_async_remote_copy(
-                        src_ref=ob.at[qs, tile(rows_at(m, cs))],
+                        src_ref=ob.at[qs, tile(rows_at(j, cs))],
                         dst_ref=rb.at[tile(ep * 16)],
-                        send_sem=ret_send.at[(m * 2 + cs) * Q + qs],
+                        send_sem=ret_send.at[(j * 2 + cs) * Q + qs],
                         recv_sem=ret_recv.at[ep],
                         device_id=(z_to * 2 + cs, place(c, qs, column)),
                         device_id_type=MESH,
                     )
-                    if m == 0 and qs == 0:
-                        own = jnp.logical_and(quarter == 0, c == cs)
+                    if qs == 0:
+                        own = is_own(j, cs)
 
                         @pl.when(jnp.logical_not(own))
                         def _():
@@ -357,35 +419,30 @@
 
                         @pl.when(own)
                         def _():
-                            rb[tile(ep * 16), :] = ob[0, tile(rows_at(0, cs)), :]
+                            rb[tile(ep * 16), :] = ob[0, tile(rows_at(j, cs)), :]
                         sends.append((copy, own))
                     else:
                         copy.start()
                         sends.append((copy, None))
 
-    far, near = 0, 1
-    await_dispatch(far)
-    x_parts[far].start()
-    await_dispatch(near)
-    x_parts[near].start()
-    x_parts[far].finish()
+    pass_rows(0)
+    pass_rows(1)
+    pass_rows(2)
+    x_parts[0].finish()
     gu.finish()
-    make_hidden(far)
-    h_parts[far].start()
+    make_hidden(0)
+    x_parts[1].finish()
+    make_hidden(1)
     dn.finish()
     for k in range(2):
         @pl.when(c == k)
         def _():
             order_down(k)
-    x_parts[near].finish()
-    make_hidden(near)
-    h_parts[near].start()
-    h_parts[far].finish()
-    make_result(far)
-    send_back(far)
-    h_parts[near].finish()
-    make_result(near)
-    send_back(near)
+    x_parts[2].finish()
+    make_hidden(2)
+    make_result(0)
+    make_result(1)
+    make_result(2)
 
     for dz in range(NZ):
         for ce in range(2):
@@ -438,9 +495,9 @@
             pltpu.VMEM((512, 128), BF16),
             pltpu.VMEM((Q, 128, D), BF16),
             pltpu.VMEM((Q, HALF, D), BF16),
-            pltpu.VMEM((256, D), BF16),
+            pltpu.VMEM((Q, 256, 256), BF16),
             pltpu.VMEM((Q, Q, 128, 128), BF16),
-            pltpu.VMEM((N_PART, Q, 2, 2 * PACKED, 128), BF16),
+            pltpu.VMEM((Q, 2, 256, 128), BF16),
             pltpu.VMEM((Q, 128, 128), BF16),
             pltpu.VMEM((512, 128), BF16),
             pltpu.VMEM((512, 768), BF16),

time: 55.7 us -> 52 us (0.934)
  Pallas kernels: 54.2 us -> 50.5 us
    pallas_call x1, Pallas kernels: 54.2 us -> 50.5 us  [body(): pl.pallas_call(kernel, out_shape=jax.ShapeDtypeStruct((HALF, TOK), BF16),...]
where the time goes in v5:
time: 52 us; the launch traced here: 51.8 us
  Pallas kernels  50.5 us (97%)
  local copies, waits for them, and re-layouts  1.32 us (3%)
    pallas_call x1, Pallas kernels, body(): pl.pallas_call(kernel, out_shape=jax.ShapeDtypeStruct((HALF, TOK), BF16),...  50.5 us
    unnamed x1, local copies, waits for them, and re-layouts  1.32 us

profile of v5, /device:TPU:1, one launch (start us, length us, event | category | flops | bytes accessed | tf_op | source)
XLA Modules:
  0.0 51.8 jit_solution(13337055611029598633)
XLA Ops:
  0.0 50.5 %shard_map.73 = bf16[64,128]{1,0:T(8,128)(2,1)} custom-call(bf16[64,128]{1,0:T(8,128)(2,1)} %bitcast.12, f32[8,128]{1,0:T(8,128)} %bitcast.13, bf16[1,64,1024]{2,1,0:T(8,128)(2,1)} %bitcast.8, bf16[1,64,1024]{2,1,0:T(8,128)(2,1)} %bitcast.9, bf16[1,64,1024]{2,1,0:T(8,128)(2,1)} %bitcast.10, s32[4,128]{1,0:T(4,128)} %bitcast.14, f32[4,128]{1,0:T(4,128)} %bitcast.15), custom_call_target="tpu_custom_call" | custom-call | tf_op jit(solution)/shard_map/pallas_call | solution.py:485
  50.5 1.3 %copy.9 = bf16[128,64]{0,1:T(8,128)(2,1)} copy(bf16[128,64]{0,1:T(8,128)(2,1)} %bitcast.11) | data formatting | bytes 32768

commit v6 on v5

--- a/solution.py
+++ b/solution.py
@@ -75,103 +75,65 @@
     return pl.ds(start if isinstance(start, int) else pl.multiple_of(start, 16), 16)
 
 
-class Gather:
-    def __init__(self, view, mine, device, sems, base):
-        self.view, self.device, self.base = view, device, base
-        self.send_sems, self.recv_sems = sems
-        self.mine = mine
-        self.right = mine + 1 - 2 * (mine % 2)
-        self.left = mine + 2 - 4 * (mine // 2)
-        self.far = 3 - mine
-        self.sent = []
-
-    def copy(self, owner, h, to, index):
-        return pltpu.make_async_remote_copy(
-            src_ref=self.view(owner, h),
-            dst_ref=self.view(owner, h),
-            send_sem=self.send_sems.at[self.base + index],
-            recv_sem=self.recv_sems.at[self.base + index],
-            device_id=self.device(to),
-            device_id_type=MESH,
-        )
-
-    def send(self, owner, h, to, index):
-        copy = self.copy(owner, h, to, index)
-        copy.start()
-        self.sent.append(copy)
-
-    def arrived(self, owner, h, index):
-        self.copy(owner, h, self.right, index).wait_recv()
-
-    def start(self):
-        self.send(self.mine, 0, self.right, 0)
-        self.send(self.mine, 1, self.left, 1)
-        self.send(self.mine, 1, self.right, 2)
-        self.send(self.mine, 0, self.left, 3)
-
-    def forward(self):
-        self.arrived(self.right, 0, 0)
-        self.send(self.right, 0, self.left, 5)
-        self.arrived(self.left, 1, 1)
-        self.send(self.left, 1, self.right, 4)
-
-    def finish(self):
-        self.arrived(self.right, 1, 2)
-        self.arrived(self.left, 0, 3)
-        self.arrived(self.far, 1, 4)
-        self.arrived(self.far, 0, 5)
-
-    def drain(self):
-        for copy in self.sent:
-            copy.wait_send()
-
-
-class Exchange:
-    def __init__(self, view, pieces, mine, device, sems, base):
-        self.view, self.device, self.base = view, device, base
-        self.pieces = pieces
-        self.send_sems, self.recv_sems = sems
+def sized(ref, sem, device):
+    return pltpu.make_async_remote_copy(
+        src_ref=ref, dst_ref=ref, send_sem=sem, recv_sem=sem, device_id=device, device_id_type=MESH
+    )
+
+
+class Square:
+    def __init__(self, view, mine, device, send_sem, recv_sems):
+        self.view, self.device = view, device
+        self.send_sem, self.recv_sems = send_sem, recv_sems
         self.mine = mine
         self.right = mine + 1 - 2 * (mine % 2)
         self.left = mine + 2 - 4 * (mine // 2)
         self.far = 3 - mine
         self.others = (self.far, self.right, self.left)
-        self.sent = []
-
-    def copy(self, owner, h, to, index):
-        return pltpu.make_async_remote_copy(
+
+    def send(self, owner, h, to, index):
+        pltpu.make_async_remote_copy(
             src_ref=self.view(owner, h),
             dst_ref=self.view(owner, h),
-            send_sem=self.send_sems.at[self.base + 3 * h + index],
-            recv_sem=self.recv_sems.at[self.base + 3 * h + index],
+            send_sem=self.send_sem,
+            recv_sem=self.recv_sems.at[index],
             device_id=self.device(to),
             device_id_type=MESH,
-        )
-
-    def send(self, h):
+        ).start()
+
+    def arrived(self, ref, index):
+        sized(ref, self.recv_sems.at[index], self.device(self.right)).wait_recv()
+
+
+class Gather(Square):
+    def start(self):
+        self.send(self.mine, 0, self.right, 0)
+        self.send(self.mine, 1, self.left, 1)
+        self.send(self.mine, 1, self.right, 2)
+        self.send(self.mine, 0, self.left, 2)
+
+    def forward(self):
+        self.arrived(self.view(self.right, 0), 0)
+        self.send(self.right, 0, self.left, 2)
+        self.arrived(self.view(self.left, 1), 1)
+        self.send(self.left, 1, self.right, 2)
+
+
+class Exchange(Square):
+    def __init__(self, *args, apart):
+        super().__init__(*args)
+        self.apart = apart
+
+    def send_all(self, h):
         for index, to in enumerate(self.others):
-            copy = self.copy(self.mine, h, to, index)
-            copy.start()
-            self.sent.append(copy)
-
-    def arrived(self, index):
-        for h in range(self.pieces):
-            self.copy(self.others[index], h, self.right, index).wait_recv()
-
-    def finish(self):
-        for index in (1, 2, 0):
-            self.arrived(index)
-
-    def drain(self):
-        for copy in self.sent:
-            copy.wait_send()
+            self.send(self.mine, h, to, index if self.apart else 0)
 
 
 def kernel(
     tok_hbm, gain_hbm, gate_hbm, up_hbm, down_hbm, ids_hbm, rw_hbm, out_ref,
     tok, gain, ids, rw,
     pbuf, gub, dnb, dnf, xb, hb, ob, rb, mixer,
-    in_sem, disp_send, disp_recv, ret_send, ret_recv, ring_send, ring_recv,
+    in_sem, disp_send, disp_recv, ret_send, ret_recv, send_sems, gu_recv, dn_recv, x_recv, h_recv,
 ):
     ep = lax.axis_index("ep")
     tp = lax.axis_index("tp")
@@ -181,16 +143,6 @@
     quarter_of, column_of = (side_b, side_a), (side_a, side_b)
     quarter = side_b + c * (side_a - side_b)
     column = side_a + c * (side_b - side_a)
-
-    loads = []
-    for i, (src, dst) in enumerate(
-        ((ids_hbm, ids), (tok_hbm, tok), (gate_hbm.at[0], gub.at[quarter, pl.ds(0, HALF)]),
-         (up_hbm.at[0], gub.at[quarter, pl.ds(HALF, HALF)]), (down_hbm.at[0], dnb.at[quarter]),
-         (gain_hbm, gain), (rw_hbm, rw))
-    ):
-        load = pltpu.make_async_copy(src, dst, in_sem.at[i])
-        load.start()
-        loads.append(load)
 
     barrier = pltpu.get_barrier_semaphore()
 
@@ -220,18 +172,31 @@
                 else:
                     greet(device)
 
-    sems = (ring_send, ring_recv)
-    gu = Gather(lambda o, h: gub.at[o, pl.ds(h * HALF, HALF)], quarter, with_column, sems, 0)
-    dn = Gather(lambda o, h: dnb.at[o, pl.ds(h * 32, 32)], quarter, with_column, sems, 6)
+    loads = []
+    for i, (src, dst) in enumerate(
+        ((ids_hbm, ids), (tok_hbm, tok), (gate_hbm.at[0], gub.at[quarter, pl.ds(0, HALF)]),
+         (up_hbm.at[0], gub.at[quarter, pl.ds(HALF, HALF)]), (down_hbm.at[0], dnb.at[quarter]),
+         (gain_hbm, gain), (rw_hbm, rw))
+    ):
+        load = pltpu.make_async_copy(src, dst, in_sem.at[i])
+        load.start()
+        loads.append(load)
+
+    gu = Gather(
+        lambda o, h: gub.at[o, pl.ds(h * HALF, HALF)], quarter, with_column, send_sems.at[0], gu_recv
+    )
+    dn = Gather(
+        lambda o, h: dnb.at[o, pl.ds(h * 32, 32)], quarter, with_column, send_sems.at[1], dn_recv
+    )
     x_parts, h_parts = [], []
     for i, part in enumerate(PARTS):
         x_parts.append(Exchange(
             lambda o, h, first=part[0]: xb.at[o, :, pl.ds((first + h) * 32, 32)],
-            len(part), column, with_quarter, sems, 12 + 12 * i,
+            column, with_quarter, send_sems.at[2], x_recv.at[pl.ds(i, 1)], apart=False,
         ))
         h_parts.append(Exchange(
             lambda o, h, part=part: hb.at[o, h, pl.ds(part[0] * 64, len(part) * 64)],
-            2, column, with_quarter, sems, 18 + 12 * i,
+            column, with_quarter, send_sems.at[3], h_recv.at[i], apart=True,
         ))
     for gather in (gu, x_parts[0]):
         greet(gather.device(gather.right))
@@ -269,8 +234,8 @@
                 copy = pltpu.make_async_remote_copy(
                     src_ref=pbuf.at[tile(e * 16)],
                     dst_ref=xb.at[column_of[ce], quarter_of[ce], tile(rows_at(z // Q, c))],
-                    send_sem=disp_send.at[dz * 2 + ce],
-                    recv_sem=disp_recv.at[(z // Q * 2 + c) * Q + quarter_of[ce]],
+                    send_sem=disp_send,
+                    recv_sem=disp_recv.at[z // Q],
                     device_id=(e, place(ce, dz % Q, column_of[ce])),
                     device_id_type=MESH,
                 )
@@ -284,18 +249,6 @@
                         xb[column, 0, tile(rows_at(z // Q, c)), :] = pbuf[tile(e * 16), :]
                 else:
                     copy.start()
-
-    sends = []
-    for dz in Z_ORDER:
-        for ce in range(2):
-            sends.append((pltpu.make_async_remote_copy(
-                src_ref=pbuf.at[tile(0)],
-                dst_ref=pbuf.at[tile(0)],
-                send_sem=disp_send.at[dz * 2 + ce],
-                recv_sem=disp_recv.at[0],
-                device_id=(ep, tp),
-                device_id_type=MESH,
-            ), is_mine(dz, ce)))
 
     dispatch()
 
@@ -319,25 +272,27 @@
     gu.forward()
     dn.forward()
 
+    def all_but_own(own, whole, rest, sem, wait):
+        @pl.when(jnp.logical_not(own))
+        def _():
+            wait(sized(whole, sem, (ep, tp)))
+
+        @pl.when(own)
+        def _():
+            wait(sized(rest, sem, (ep, tp)))
+
     def pass_rows(part):
         for h, j in enumerate(PARTS[part]):
-            for cs in range(2):
-                for qs in range(Q):
-                    arrived = pltpu.make_async_remote_copy(
-                        src_ref=pbuf.at[tile(0)],
-                        dst_ref=xb.at[column, qs, tile(rows_at(j, cs))],
-                        send_sem=disp_send.at[0],
-                        recv_sem=disp_recv.at[(j * 2 + cs) * Q + qs],
-                        device_id=(ep, tp),
-                        device_id_type=MESH,
-                    )
-                    if qs == 0:
-                        @pl.when(jnp.logical_not(is_own(j, cs)))
-                        def _():
-                            arrived.wait_recv()
-                    else:
-                        arrived.wait_recv()
-            x_parts[part].send(h)
+            all_but_own(
+                jnp.logical_and(quarter == 0, z // Q == j),
+                xb.at[column, :, pl.ds(j * 32, 32)], pbuf.at[pl.ds(0, 112)],
+                disp_recv.at[j], lambda copy: copy.wait_recv(),
+            )
+            x_parts[part].send_all(h)
+
+    def x_arrived(part):
+        js = PARTS[part]
+        x_parts[part].arrived(xb.at[pl.ds(0, 3), :, pl.ds(js[0] * 32, len(js) * 32)], 0)
 
     def slice_at(s, part):
         (ty, uy), (tx, ux) = bits(s // Q), bits(s % Q)
@@ -365,7 +320,7 @@
             up_pre = jnp.clip(up_pre, -LIMIT, LIMIT)
             hidden = (up_pre + 1.0) * gate_pre * jax.nn.sigmoid(ALPHA * gate_pre)
             hb[column, p, at : at + count] = hidden.astype(BF16)
-            h_parts[part].send(p)
+            h_parts[part].send_all(p)
 
     def order_down(k):
         low = iota((HALF, 128), 1) < HALF
@@ -389,8 +344,9 @@
 
         result = term(column)
         for index in (1, 2, 0):
-            exchange.arrived(index)
-            result = result + term(exchange.others[index])
+            owner = exchange.others[index]
+            exchange.arrived(hb.at[owner, :, pl.ds(2 * at, 2 * count)], index)
+            result = result + term(owner)
         for n in range(2):
             cols = result[:, n * 128 : n * 128 + 128]
             pair = swap(cols[:count], cols[count:])
@@ -405,8 +361,8 @@
                     copy = pltpu.make_async_remote_copy(
                         src_ref=ob.at[qs, tile(rows_at(j, cs))],
                         dst_ref=rb.at[tile(ep * 16)],
-                        send_sem=ret_send.at[(j * 2 + cs) * Q + qs],
-                        recv_sem=ret_recv.at[ep],
+                        send_sem=ret_send,
+                        recv_sem=ret_recv,
                         device_id=(z_to * 2 + cs, place(c, qs, column)),
                         device_id_type=MESH,
                     )
@@ -420,47 +376,31 @@
                         @pl.when(own)
                         def _():
                             rb[tile(ep * 16), :] = ob[0, tile(rows_at(j, cs)), :]
-                        sends.append((copy, own))
                     else:
                         copy.start()
-                        sends.append((copy, None))
 
     pass_rows(0)
     pass_rows(1)
     pass_rows(2)
-    x_parts[0].finish()
-    gu.finish()
+    x_arrived(0)
+    gu.arrived(gub.at[pl.ds(0, 2)], 2)
     make_hidden(0)
-    x_parts[1].finish()
+    x_arrived(1)
     make_hidden(1)
-    dn.finish()
+    dn.arrived(dnb.at[pl.ds(0, 2)], 2)
     for k in range(2):
         @pl.when(c == k)
         def _():
             order_down(k)
-    x_parts[2].finish()
+    x_arrived(2)
     make_hidden(2)
     make_result(0)
     make_result(1)
     make_result(2)
 
-    for dz in range(NZ):
-        for ce in range(2):
-            e = ((z + dz) % NZ) * 2 + ce
-            arrived = pltpu.make_async_remote_copy(
-                src_ref=ob.at[0, tile(0)],
-                dst_ref=rb.at[tile(e * 16)],
-                send_sem=ret_send.at[0],
-                recv_sem=ret_recv.at[e],
-                device_id=(ep, tp),
-                device_id_type=MESH,
-            )
-            if dz == 0:
-                @pl.when(jnp.logical_not(jnp.logical_and(quarter_of[ce] == 0, c == ce)))
-                def _():
-                    arrived.wait_recv()
-            else:
-                arrived.wait_recv()
+    all_but_own(
+        quarter == 0, rb, rb.at[pl.ds(0, 496)], ret_recv, lambda copy: copy.wait_recv()
+    )
 
     mixed = dot_columns(rb[...], mixer[...])
     combined = mixed[0:HALF, 0:128] + mixed[HALF:128, 384:512]
@@ -469,22 +409,17 @@
         combined = combined + mixed[HALF:128, 384 + i * 128 : 512 + i * 128]
     out_ref[...] = combined.astype(BF16)
 
-    for copy, own in sends:
-        if own is None:
-            copy.wait_send()
-        else:
-            @pl.when(jnp.logical_not(own))
-            def _():
-                copy.wait_send()
-    for gather in [gu, dn] + x_parts + h_parts:
-        gather.drain()
+    for sem in (disp_send, ret_send):
+        all_but_own(quarter == 0, rb, rb.at[pl.ds(0, 496)], sem, lambda copy: copy.wait_send())
+    for i, buf in enumerate((gub, dnb, xb, hb)):
+        sized(buf.at[pl.ds(0, 3)], send_sems.at[i], (ep, tp)).wait_send()
 
 
 def body(tokens, norm_gain, gate_weight, up_weight, down_weight, expert_ids, route_weight):
     turned = (0, 2, 1)
     return pl.pallas_call(
         kernel,
-        out_shape=jax.ShapeDtypeStruct((HALF, TOK), BF16),
+        out_shape=pltpu.VMEM((HALF, TOK), BF16),
         in_specs=[pl.BlockSpec(memory_space=pl.ANY)] * 7,
         out_specs=pl.BlockSpec(memory_space=pltpu.VMEM),
         scratch_shapes=[
@@ -502,12 +437,15 @@
             pltpu.VMEM((512, 128), BF16),
             pltpu.VMEM((512, 768), BF16),
             pltpu.SemaphoreType.DMA((7,)),
-            pltpu.SemaphoreType.DMA((32,)),
-            pltpu.SemaphoreType.DMA((32,)),
-            pltpu.SemaphoreType.DMA((32,)),
-            pltpu.SemaphoreType.DMA((32,)),
-            pltpu.SemaphoreType.DMA((12 + 12 * N_PART,)),
-            pltpu.SemaphoreType.DMA((12 + 12 * N_PART,)),
+            pltpu.SemaphoreType.DMA,
+            pltpu.SemaphoreType.DMA((Q,)),
+            pltpu.SemaphoreType.DMA,
+            pltpu.SemaphoreType.DMA,
+            pltpu.SemaphoreType.DMA((4,)),
+            pltpu.SemaphoreType.DMA((3,)),
+            pltpu.SemaphoreType.DMA((3,)),
+            pltpu.SemaphoreType.DMA((N_PART,)),
+            pltpu.SemaphoreType.DMA((N_PART, 3)),
         ],
         compiler_params=pltpu.CompilerParams(collective_id=0, has_side_effects=True),
     )(

time: 52 us -> 47.8 us (0.919)
  Pallas kernels: 50.5 us -> 47.1 us
  local copies, waits for them, and re-layouts: 1.32 us -> 0.61 us
    pallas_call x1, Pallas kernels: 50.5 us -> 47.1 us  [body(): pl.pallas_call(kernel, out_shape=pltpu.VMEM((HALF, TOK), BF16), in_specs=...]
    unnamed x1, local copies, waits for them, and re-layouts: 1.32 us -> 0.61 us
where the time goes in v6:
time: 47.8 us; the launch traced here: 47.7 us
  Pallas kernels  47.1 us (99%)
  local copies, waits for them, and re-layouts  0.61 us (1%)
    pallas_call x1, Pallas kernels, body(): pl.pallas_call(kernel, out_shape=pltpu.VMEM((HALF, TOK), BF16), in_specs=...  47.1 us

profile of v6, /device:TPU:1, one launch (start us, length us, event | category | flops | bytes accessed | tf_op | source)
XLA Modules:
  0.0 47.7 jit_solution(6863875495991847896)
XLA Ops:
  0.0 47.1 %shard_map.73 = bf16[64,128]{1,0:T(8,128)(2,1)S(1)} custom-call(bf16[64,128]{1,0:T(8,128)(2,1)} %bitcast.12, f32[8,128]{1,0:T(8,128)} %bitcast.13, bf16[1,64,1024]{2,1,0:T(8,128)(2,1)} %bitcast.9, bf16[1,64,1024]{2,1,0:T(8,128)(2,1)} %bitcast.10, bf16[1,64,1024]{2,1,0:T(8,128)(2,1)} %bitcast.11, s32[4,128]{1,0:T(4,128)} %bitcast.14, f32[4,128]{1,0:T(4,128)} %bitcast.15), custom_call_target="tpu_custom_call" | custom-call | tf_op jit(solution)/shard_map/pallas_call | solution.py:420
  47.1 0.6 %copy.9 = bf16[128,64]{0,1:T(8,128)(2,1)} copy(bf16[128,64]{0,1:T(8,128)(2,1)S(1)} %bitcast.8) | data formatting | bytes 32768

commit v7 on v6

--- a/solution.py
+++ b/solution.py
@@ -20,6 +20,7 @@
 EXPERTS = 32
 TOPK = 4
 HALF = 64
+LATE_FROM = 8
 Z_ORDER = (8, 7, 9, 6, 10, 5, 11, 4, 12, 3, 13, 2, 14, 1, 15, 0)
 PARTS = ((0,), (1,), (2, 3))
 N_PART = len(PARTS)
@@ -250,7 +251,7 @@
                 else:
                     copy.start()
 
-    dispatch()
+    pl.when(z < LATE_FROM)(dispatch)
 
     for load in loads[2:5]:
         load.wait()
@@ -269,6 +270,7 @@
         mixer[:, i * 128 : i * 128 + 128] = (wide * pick_low).astype(BF16)
         mixer[:, 384 + i * 128 : 512 + i * 128] = (wide * pick_high).astype(BF16)
 
+    pl.when(z >= LATE_FROM)(dispatch)
     gu.forward()
     dn.forward()
 
@@ -392,9 +394,9 @@
         @pl.when(c == k)
         def _():
             order_down(k)
+    make_result(0)
     x_arrived(2)
     make_hidden(2)
-    make_result(0)
     make_result(1)
     make_result(2)
 

time: 47.8 us -> 48.1 us (level)
  the two profiles are of different devices: /device:TPU:1 before, /device:TPU:83 now
where the time goes in v7:
time: 48.1 us; the launch traced here: 48 us
  Pallas kernels  47.4 us (99%)
  local copies, waits for them, and re-layouts  0.61 us (1%)
    pallas_call x1, Pallas kernels, body(): pl.pallas_call(kernel, out_shape=pltpu.VMEM((HALF, TOK), BF16), in_specs=...  47.4 us

profile of v7, /device:TPU:83, one launch (start us, length us, event | category | flops | bytes accessed | tf_op | source)
XLA Modules:
  0.0 48.0 jit_solution(18065982538727843075)
XLA Ops:
  0.0 47.4 %shard_map.73 = bf16[64,128]{1,0:T(8,128)(2,1)S(1)} custom-call(bf16[64,128]{1,0:T(8,128)(2,1)} %bitcast.12, f32[8,128]{1,0:T(8,128)} %bitcast.13, bf16[1,64,1024]{2,1,0:T(8,128)(2,1)} %bitcast.9, bf16[1,64,1024]{2,1,0:T(8,128)(2,1)} %bitcast.10, bf16[1,64,1024]{2,1,0:T(8,128)(2,1)} %bitcast.11, s32[4,128]{1,0:T(4,128)} %bitcast.14, f32[4,128]{1,0:T(4,128)} %bitcast.15), custom_call_target="tpu_custom_call" | custom-call | tf_op jit(solution)/shard_map/pallas_call | solution.py:422
  47.4 0.6 %copy.9 = bf16[128,64]{0,1:T(8,128)(2,1)} copy(bf16[128,64]{0,1:T(8,128)(2,1)S(1)} %bitcast.8) | data formatting | bytes 32768

commit v8 on v6

--- a/solution.py
+++ b/solution.py
@@ -382,16 +382,16 @@
     pass_rows(0)
     pass_rows(1)
     pass_rows(2)
+    dn.arrived(dnb.at[pl.ds(0, 2)], 2)
+    for k in range(2):
+        @pl.when(c == k)
+        def _():
+            order_down(k)
     x_arrived(0)
     gu.arrived(gub.at[pl.ds(0, 2)], 2)
     make_hidden(0)
     x_arrived(1)
     make_hidden(1)
-    dn.arrived(dnb.at[pl.ds(0, 2)], 2)
-    for k in range(2):
-        @pl.when(c == k)
-        def _():
-            order_down(k)
     x_arrived(2)
     make_hidden(2)
     make_result(0)

time: 47.8 us -> 47.9 us (level)
  no operation moved by 1% of the time
where the time goes in v8:
time: 47.9 us; the launch traced here: 47.7 us
  Pallas kernels  47.1 us (98%)
  local copies, waits for them, and re-layouts  0.61 us (1%)
    pallas_call x1, Pallas kernels, body(): pl.pallas_call(kernel, out_shape=pltpu.VMEM((HALF, TOK), BF16), in_specs=...  47.1 us

profile of v8, /device:TPU:1, one launch (start us, length us, event | category | flops | bytes accessed | tf_op | source)
XLA Modules:
  0.0 47.7 jit_solution(11313105225927695651)
XLA Ops:
  0.0 47.1 %shard_map.73 = bf16[64,128]{1,0:T(8,128)(2,1)S(1)} custom-call(bf16[64,128]{1,0:T(8,128)(2,1)} %bitcast.12, f32[8,128]{1,0:T(8,128)} %bitcast.13, bf16[1,64,1024]{2,1,0:T(8,128)(2,1)} %bitcast.9, bf16[1,64,1024]{2,1,0:T(8,128)(2,1)} %bitcast.10, bf16[1,64,1024]{2,1,0:T(8,128)(2,1)} %bitcast.11, s32[4,128]{1,0:T(4,128)} %bitcast.14, f32[4,128]{1,0:T(4,128)} %bitcast.15), custom_call_target="tpu_custom_call" | custom-call | tf_op jit(solution)/shard_map/pallas_call | solution.py:420
  47.1 0.6 %copy.9 = bf16[128,64]{0,1:T(8,128)(2,1)} copy(bf16[128,64]{0,1:T(8,128)(2,1)S(1)} %bitcast.8) | data formatting | bytes 32768
